TPU v7x, 256 devices: a whole 4x4x8 slice. The times are simulated.
256 devices in a mesh: ep: 16 (over y, x), tp: 16 (over z, core).
Axes of the slice: x: 4, y: 4, z: 8, core: 2. Of those that a mesh axis runs over, the one named last changes fastest.
Arguments:
- residual: bfloat16 [1024, 2048], P('ep'), may hold values from -20 to 20
- cache_latent: bfloat16 [1024, 2048, 256], P(('ep', 'tp')), may hold values from -12 to 12
- cache_rope: bfloat16 [1024, 32, 2048], P(('ep', 'tp')), may hold values from -6 to 6
- lengths: int32 [1024], P(('ep', 'tp')), may hold values from 2 to 2048, as said below
- query_latent: bfloat16 [1024, 32, 256], P(('ep', 'tp')), may hold values from -250 to 250
- query_rope: bfloat16 [1024, 32, 32], P(('ep', 'tp')), may hold values from -6 to 6
- norm_gain: bfloat16 [2048], replicated, may hold values from 0.099609375 to 1.8984375
- latent_weight: bfloat16 [2048, 256], replicated, may hold values from -0.125 to 0.125
- latent_gain: bfloat16 [256], replicated, may hold values from 0.099609375 to 1.8984375
- rope_weight: bfloat16 [32, 2048], replicated, may hold values from -0.125 to 0.125
- value_weight: bfloat16 [256, 2048], replicated, may hold values from -0.375 to 0.375
- out_weight: bfloat16 [2048, 2048], P('tp'), may hold values from -1 to 1
- mixer_gain: bfloat16 [2048], replicated, may hold values from 0.099609375 to 1.8984375
- group_router: bfloat16 [2048, 4], replicated, may hold values from -0.0625 to 0.0625
- expert_router: bfloat16 [2048, 32], replicated, may hold values from -0.0625 to 0.0625
- expert_ids: int32 [1024, 2], P('ep'), may hold values from 0 to 31, as said below
- gate_weight: bfloat16 [32, 2048, 4096], P('ep', None, 'tp'), may hold values from -0.125 to 0.125
- up_weight: bfloat16 [32, 2048, 4096], P('ep', None, 'tp'), may hold values from -0.125 to 0.125
- down_weight: bfloat16 [32, 4096, 2048], P('ep', 'tp'), may hold values from -0.75 to 0.75
Outputs:
- mixed: bfloat16 [1024, 2048], P('ep')
- new_latent: bfloat16 [1024, 256], P(('ep', 'tp'))
- new_rope_key: bfloat16 [1024, 32], P(('ep', 'tp'))
Inputs may be any that keep to these rules, and one draw needn't show every extreme that they name: `lengths`: every sequence has 2 or more cached positions, and in every draw some sequence has all 2048. `expert_ids`: each row names 2 different experts of one group; group g holds experts g * 8 to g * 8 + 7. Among the rows of one index of ep (aligned blocks of 64 rows) no expert is named more than 8 times, and in every draw some expert is named exactly 8 times in every block.
All inputs are finite; a program needn't handle non-finite values.
Results may differ from a plain program's by a relative error of at most 0.012.
Values may be sent and summed in bfloat16 or wider, within the bound.
A program may use at most 64 MiB of HBM per device.

v0:
```python
import jax
import jax.numpy as jnp
from jax import lax
from jax.sharding import PartitionSpec as P

H = 32
KV = 256
ROPE = 32
NOPE = 64
V = 64
GROUPS = 4
TOPK = 2


NORM_EPSILON = 1e-06
ROPE_BASE = 10000.0


def cut_along(value, dim, peers):
    before, after = (value.shape[:dim], value.shape[dim + 1 :])
    return jnp.moveaxis(value.reshape(*before, peers, -1, *after), dim, 0)


def sent_and_summed(value, axis, dim):
    tiles = cut_along(value, dim, lax.axis_size(axis))
    arrived = lax.all_to_all(tiles, axis, split_axis=0, concat_axis=0, tiled=True)
    return arrived.sum(axis=0)


def inverse_rms(values):
    return lax.rsqrt(jnp.mean(values * values, axis=-1, keepdims=True) + NORM_EPSILON)


def rotate(vector, position):
    half_width = vector.shape[-1] // 2
    frequency = ROPE_BASE ** (
        -jnp.arange(0, vector.shape[-1], 2, dtype=jnp.float32) / vector.shape[-1]
    )
    angles = position[..., None] * frequency
    lower_half = vector[..., :half_width]
    upper_half = vector[..., half_width:]
    return jnp.concatenate(
        [
            lower_half * jnp.cos(angles) - upper_half * jnp.sin(angles),
            upper_half * jnp.cos(angles) + lower_half * jnp.sin(angles),
        ],
        axis=-1,
    )


def dispatch_table(expert_rows, experts, capacity):
    flat_ids = expert_rows.reshape(-1)
    hit_table = (flat_ids[:, None] == jnp.arange(experts, dtype=jnp.int32)[None, :]).astype(
        jnp.int32
    )
    slot_rank = jnp.sum((jnp.cumsum(hit_table, axis=0) - hit_table) * hit_table, axis=1)
    slot_index = flat_ids * capacity + slot_rank
    picked = (
        slot_index[None, :] == jnp.arange(experts * capacity, dtype=jnp.int32)[:, None]
    ).astype(jnp.float32)
    return picked.reshape(experts * capacity, expert_rows.shape[0], expert_rows.shape[1])


def route_weights(expert_in, group_router, expert_router, expert_ids, per_group):
    group_logits = jnp.dot(expert_in, group_router, preferred_element_type=jnp.float32)
    expert_logits = jnp.dot(expert_in, expert_router, preferred_element_type=jnp.float32)
    chosen = expert_ids[:, 0] // per_group
    group_hit = (
        jnp.arange(group_logits.shape[1], dtype=jnp.int32)[None, :] == chosen[:, None]
    ).astype(jnp.float32)
    chosen_logit = jnp.sum(group_logits * group_hit, axis=1, keepdims=True)
    group_share = 1.0 / jnp.sum(jnp.exp(group_logits - chosen_logit), axis=1)
    expert_hit = (
        expert_ids[:, :, None] == jnp.arange(expert_logits.shape[1], dtype=jnp.int32)[None, None, :]
    ).astype(jnp.float32)
    picked_logit = jnp.sum(expert_hit * expert_logits[:, None, :], axis=2)
    inner_share = 1.0 / jnp.sum(
        jnp.exp(picked_logit[:, None, :] - picked_logit[:, :, None]), axis=2
    )
    return group_share[:, None] * inner_share


def on_device(
    residual,
    cache_latent,
    cache_rope,
    lengths,
    query_latent,
    query_rope,
    norm_gain,
    latent_weight,
    latent_gain,
    rope_weight,
    value_weight,
    out_weight,
    mixer_gain,
    group_router,
    expert_router,
    expert_ids,
    gate_weight,
    up_weight,
    down_weight,
):
    ep_count = lax.axis_size("ep")
    seq_count = cache_latent.shape[0]
    group_rows = residual.shape[0]
    model_width = residual.shape[1]
    resid_f = residual.astype(jnp.float32)
    own_rows = lax.dynamic_slice_in_dim(resid_f, lax.axis_index("tp") * seq_count, seq_count, 0)
    normed = (own_rows * inverse_rms(own_rows) * norm_gain.astype(jnp.float32)).astype(jnp.bfloat16)
    latent_raw = jnp.dot(normed, latent_weight, preferred_element_type=jnp.float32)
    new_latent = (latent_raw * inverse_rms(latent_raw) * latent_gain.astype(jnp.float32)).astype(
        jnp.bfloat16
    )
    positions = lengths.astype(jnp.float32)
    rope_raw = jnp.dot(normed, rope_weight.T, preferred_element_type=jnp.float32)
    new_rope_key = rotate(rope_raw, positions).astype(jnp.bfloat16)
    query_turned = rotate(query_rope.astype(jnp.float32), positions[:, None]).astype(jnp.bfloat16)
    score_scale = (NOPE + ROPE) ** (-0.5)
    cached = (
        jnp.einsum("shc,spc->shp", query_latent, cache_latent, preferred_element_type=jnp.float32)
        + jnp.einsum("shr,srp->shp", query_turned, cache_rope, preferred_element_type=jnp.float32)
    ) * score_scale
    keeping = (
        jnp.arange(cache_latent.shape[1], dtype=jnp.int32)[None, None, :] < lengths[:, None, None]
    )
    cached = jnp.where(keeping, cached, -jnp.inf)
    fresh = (
        jnp.einsum("shc,sc->sh", query_latent, new_latent, preferred_element_type=jnp.float32)
        + jnp.einsum("shr,sr->sh", query_turned, new_rope_key, preferred_element_type=jnp.float32)
    ) * score_scale
    row_top = jnp.maximum(jnp.max(cached, axis=2), fresh)
    cached_exp = jnp.exp(cached - row_top[:, :, None])
    fresh_exp = jnp.exp(fresh - row_top)
    denominator = jnp.sum(cached_exp, axis=2) + fresh_exp
    cached_weight = (cached_exp / denominator[:, :, None]).astype(jnp.bfloat16)
    fresh_weight = (fresh_exp / denominator).astype(jnp.bfloat16)
    mixed_latent = (
        jnp.einsum("shp,spc->shc", cached_weight, cache_latent, preferred_element_type=jnp.float32)
        + fresh_weight.astype(jnp.float32)[:, :, None] * new_latent.astype(jnp.float32)[:, None, :]
    ).astype(jnp.bfloat16)
    head_values = jnp.einsum(
        "shc,chv->shv",
        mixed_latent,
        value_weight.reshape(KV, H, V),
        preferred_element_type=jnp.float32,
    ).astype(jnp.bfloat16)
    by_heads = lax.all_to_all(head_values, "tp", split_axis=1, concat_axis=0, tiled=True)
    head_terms = jnp.dot(
        by_heads.reshape(group_rows, -1), out_weight, preferred_element_type=jnp.float32
    )
    attended_share = sent_and_summed(head_terms, "tp", 1)
    share_width = attended_share.shape[1]
    resid_cols = lax.dynamic_slice_in_dim(
        resid_f, lax.axis_index("tp") * share_width, share_width, 1
    )
    after_share = (resid_cols + attended_share).astype(jnp.bfloat16)
    after_attention = lax.all_gather(after_share, "tp", axis=1, tiled=True)
    after_f = after_attention.astype(jnp.float32)
    expert_in = (after_f * inverse_rms(after_f) * mixer_gain.astype(jnp.float32)).astype(
        jnp.bfloat16
    )
    experts = expert_router.shape[1]
    capacity = 2 * group_rows * TOPK // experts
    route_weight = route_weights(
        expert_in, group_router, expert_router, expert_ids, experts // GROUPS
    )
    picked = dispatch_table(expert_ids, experts, capacity)
    select_rows = jnp.sum(picked, axis=2).astype(jnp.bfloat16)
    outbound = jnp.dot(select_rows, expert_in, preferred_element_type=jnp.float32).astype(
        jnp.bfloat16
    )
    outbound = outbound.reshape(ep_count, gate_weight.shape[0], capacity, model_width)
    rows = lax.all_to_all(outbound, "ep", split_axis=0, concat_axis=0, tiled=True)
    gate_value = jnp.einsum("secd,edf->secf", rows, gate_weight, preferred_element_type=jnp.float32)
    up_value = jnp.einsum("secd,edf->secf", rows, up_weight, preferred_element_type=jnp.float32)
    activation = (jax.nn.silu(gate_value) * up_value).astype(jnp.bfloat16)
    expert_terms = jnp.einsum(
        "secf,efd->secd", activation, down_weight, preferred_element_type=jnp.float32
    )
    combine = jnp.sum(picked * route_weight[None, :, :], axis=2).T
    summed_terms = sent_and_summed(expert_terms, "tp", 3)
    returned_terms = lax.all_to_all(summed_terms, "ep", split_axis=0, concat_axis=0, tiled=True)
    share_width = returned_terms.shape[3]
    moe_part = jnp.dot(combine, returned_terms.reshape(-1, share_width))
    after_cols = lax.dynamic_slice_in_dim(
        after_f, lax.axis_index("tp") * share_width, share_width, 1
    )
    mixed_share = (after_cols + moe_part).astype(jnp.bfloat16)
    mixed = lax.all_gather(mixed_share, "tp", axis=1, tiled=True)
    return (mixed, new_latent, new_rope_key)


def solution(mesh):
    in_specs = (
        P("ep", None),
        P(("ep", "tp"), None, None),
        P(("ep", "tp"), None, None),
        P(("ep", "tp")),
        P(("ep", "tp"), None, None),
        P(("ep", "tp"), None, None),
        P(),
        P(),
        P(),
        P(),
        P(),
        P("tp", None),
        P(),
        P(),
        P(),
        P("ep", None),
        P("ep", None, "tp"),
        P("ep", None, "tp"),
        P("ep", "tp", None),
    )
    out_specs = (P("ep", None), P(("ep", "tp"), None), P(("ep", "tp"), None))
    return jax.shard_map(
        on_device, mesh=mesh, in_specs=in_specs, out_specs=out_specs, check_vma=False
    )
```

profile of v0, /device:TPU:1, one launch (start us, length us, event | category | flops | bytes accessed | tf_op | source)
XLA Modules:
  0.0 190.4 jit_solution(8067165427996181591)
XLA Ops:
  0.6 0.0 copy-start
  0.7 1.3 convert_element_type.79
  2.0 0.7 iota_compare_fusion.3
  2.7 0.0 copy-start.5
  2.8 1.5 copy.96
  4.3 0.8 convert_element_type.78
  5.0 0.8 convert_element_type.77
  5.9 1.0 multiply_reduce_fusion.1
  6.9 0.7 convert_element_type.82
  7.5 1.1 fusion.55
  8.7 1.7 multiply_reduce_fusion.2
  10.4 0.0 copy-start.10
  10.4 0.0 copy-start.3
  10.4 0.0 copy-start.1
  10.4 3.6 %fusion.64 = f32[4,32,2048]{2,1,0:T(8,128)S(1)} fusion(bf16[4,32,256]{2,1,0:T(8,128)(2,1)S(1)} %copy-done.5, bf16[4,2048,256]{2,1,0:T(8,128)(2,1)} %param.20), kind=kOutput, calls=%fused_computation.98 | convolution fusion | flops 134217728 | bytes 5308416 | tf_op jit(solution)/shard_map/shc,spc->shp/dot_general | solution.py:121
  14.0 0.1 fusion.59
  14.1 0.1 fusion.45
  14.2 0.1 subtract_convert_fusion.1
  14.4 0.1 fusion.80
  14.5 0.1 subtract_convert_fusion
  14.6 0.2 fusion.44
  14.8 0.5 fusion.60
  15.2 0.3 fusion.26
  15.6 0.9 fusion.23
  16.5 0.0 copy-start.6
  16.5 0.4 fusion.61
  16.8 0.7 reshape.202
  17.6 10.0 %all-to-all-start = ((bf16[16,2,256]{2,1,0:T(2,128)(2,1)}), bf16[16,2,256]{2,1,0:T(2,128)(2,1)S(1)}, u32[]{:S(2)}, u32[]{:S(2)}) async-start(bf16[16,2,256]{2,1,0:T(2,128)(2,1)} %reshape.202), calls=%async_computation | async-start | bytes 32768 | tf_op jit(solution)/shard_map/all_to_all | solution.py:148
  27.5 1.3 copy.114
  28.9 0.0 copy-start.11
  28.9 6.0 %all-to-all-done = bf16[16,2,256]{2,1,0:T(2,128)(2,1)S(1)} async-done(((bf16[16,2,256]{2,1,0:T(2,128)(2,1)}), bf16[16,2,256]{2,1,0:T(2,128)(2,1)S(1)}, u32[]{:S(2)}, u32[]{:S(2)}) %all-to-all-start) | async-done | bytes 16416 | tf_op jit(solution)/shard_map/all_to_all | solution.py:148
  34.9 0.1 reshape.203
  35.0 0.1 reshape.197
  35.1 0.0 copy-start.12
  35.1 1.1 convolution_bitcast_fusion
  36.2 3.7 %all-to-all-start.1 = ((f32[16,64,128]{2,1,0:T(8,128)}), f32[16,64,128]{2,1,0:T(8,128)S(1)}, u32[]{:S(2)}, u32[]{:S(2)}) async-start(f32[16,64,128]{2,1,0:T(8,128)} %convolution_bitcast_fusion), calls=%async_computation.1 | async-start | bytes 1048576 | tf_op jit(solution)/shard_map/all_to_all | solution.py:26
  40.0 0.1 copy.100
  40.1 0.1 eq.57
  40.2 0.1 fusion.42
  40.3 0.2 reduce_window_sum.11
  40.5 0.2 select_reduce_fusion.1
  40.7 0.1 reduce_sum.124
  40.8 0.1 copy.101
  40.9 16.4 %all-to-all-done.1 = f32[16,64,128]{2,1,0:T(8,128)S(1)} async-done(((f32[16,64,128]{2,1,0:T(8,128)}), f32[16,64,128]{2,1,0:T(8,128)S(1)}, u32[]{:S(2)}, u32[]{:S(2)}) %all-to-all-start.1) | async-done | bytes 524320 | tf_op jit(solution)/shard_map/all_to_all | solution.py:26
  57.3 0.8 add_convert_fusion.1
  58.1 15.2 %all_gather.6 = bf16[64,2048]{1,0:T(8,128)(2,1)S(1)} all-gather(bf16[64,128]{1,0:T(8,128)(2,1)S(1)} %add_convert_fusion.1), channel_id=1, replica_groups=mesh['ep'=16,'tp'=16] {'tp'}, dimensions={1}, use_global_device_ids=true | all-gather | bytes 278528 | tf_op jit(solution)/shard_map/all_gather | solution.py:158
  73.2 0.2 multiply_reduce_fusion
  73.4 0.3 fusion.57
  73.8 0.3 select_reduce_fusion.3
  74.1 0.1 convert_reduce_fusion
  74.2 0.5 convolution_convert_fusion
  74.7 23.1 %all_to_all.35 = bf16[16,2,8,2048]{3,2,1,0:T(8,128)(2,1)S(1)} all-to-all(bf16[16,2,8,2048]{3,2,1,0:T(8,128)(2,1)S(1)} %bitcast.87), channel_id=1, replica_groups=mesh['ep'=16,'tp'=16] {'ep'}, dimensions={0} | all-to-all | bytes 2097152 | tf_op jit(solution)/shard_map/all_to_all | solution.py:174
  97.8 1.2 fusion.11
  98.9 3.8 %fusion.8 = f32[16,2,8,16,128]{4,2,3,0,1:T(8,128)} fusion(bf16[2,256,2048]{2,1,0:T(8,128)(2,1)S(1)} %copy-done, bf16[2,2048,256]{2,1,0:T(8,128)(2,1)} %param.36, bf16[16,2,8,2048]{3,2,1,0:T(8,128)(2,1)S(1)} %all_to_all.35, f32[16,2,8,256]{3,2,0,1:T(8,128)} %fusion.11), kind=kOutput, calls=%fused_computation.11 | convolution fusion | flops 537264128 | bytes 7602176 | tf_op jit(solution)/shard_map/secf,efd->secd/dot_general | solution.py:178
  102.7 1.8 copy.131
  104.6 57.4 %all_to_all.36 = f32[16,16,2,8,128]{4,3,1,2,0:T(8,128)} all-to-all(f32[16,16,2,8,128]{4,3,1,2,0:T(8,128)S(1)} %bitcast.85), channel_id=1, replica_groups=mesh['ep'=16,'tp'=16] {'tp'}, dimensions={0} | all-to-all | bytes 4194304 | tf_op jit(solution)/shard_map/all_to_all | solution.py:26
  161.9 1.7 reduce_sum.132
  163.6 0.6 copy.106
  164.3 3.5 %all-to-all-start.4 = ((bf16[16,2,8,128]{3,2,1,0:T(8,128)(2,1)}), bf16[16,2,8,128]{3,2,1,0:T(8,128)(2,1)S(1)}, u32[]{:S(2)}, u32[]{:S(2)}) async-start(bf16[16,2,8,128]{3,2,1,0:T(8,128)(2,1)} %copy.106), calls=%async_computation.4 | async-start | bytes 131072 | tf_op jit(solution)/shard_map/all_to_all | solution.py:183
  167.8 0.6 pad_maximum_fusion.3
  168.4 5.8 %all-to-all-done.4 = bf16[16,2,8,128]{3,2,1,0:T(8,128)(2,1)S(1)} async-done(((bf16[16,2,8,128]{3,2,1,0:T(8,128)(2,1)}), bf16[16,2,8,128]{3,2,1,0:T(8,128)(2,1)S(1)}, u32[]{:S(2)}, u32[]{:S(2)}) %all-to-all-start.4) | async-done | bytes 65568 | tf_op jit(solution)/shard_map/all_to_all | solution.py:183
  174.2 0.1 fusion.25
  174.4 15.4 %all_gather.7 = bf16[64,2048]{1,0:T(8,128)(2,1)S(1)} all-gather(bf16[64,128]{1,0:T(8,128)(2,1)S(1)} %fusion.25), channel_id=1, replica_groups=mesh['ep'=16,'tp'=16] {'tp'}, dimensions={1}, use_global_device_ids=true | all-gather | bytes 278528 | tf_op jit(solution)/shard_map/all_gather | solution.py:190
  189.7 0.7 copy.133
  (36 shorter events, 0.3 us)
Async XLA Ops:
  0.6 98.3 %copy-start = (bf16[2,256,2048]{2,1,0:T(8,128)(2,1)S(1)}, bf16[2,256,2048]{2,1,0:T(8,128)(2,1)}, u32[]{:S(2)}) copy-start(bf16[2,256,2048]{2,1,0:T(8,128)(2,1)} %param.37) | copy-start | bytes 6291460
  0.6 4.4 %copy-start.4 = (bf16[64,2048]{1,0:T(8,128)(2,1)S(1)}, bf16[64,2048]{1,0:T(8,128)(2,1)}, u32[]{:S(2)}) copy-start(bf16[64,2048]{1,0:T(8,128)(2,1)} %param.19) | copy-start | bytes 786436
  0.7 5.2 %copy-start.7 = (bf16[2048]{0:T(1024)(128)(2,1)S(1)}, bf16[2048]{0:T(1024)(128)(2,1)}, u32[]{:S(2)}) copy-start(bf16[2048]{0:T(1024)(128)(2,1)} %param.25) | copy-start | bytes 12292
  2.7 7.6 %copy-start.5 = (bf16[4,32,256]{2,1,0:T(8,128)(2,1)S(1)}, bf16[4,32,256]{2,1,0:T(8,128)(2,1)}, u32[]{:S(2)}) copy-start(bf16[4,32,256]{2,1,0:T(8,128)(2,1)} %param.23) | copy-start | bytes 196612
  10.4 3.9 %copy-start.10 = (f32[4]{0:T(128)S(1)}, f32[4]{0:T(128)}, u32[]{:S(2)}) copy-start(f32[4]{0:T(128)} %convert_element_type.79) | copy-start | bytes 52
  10.4 4.4 %copy-start.3 = (bf16[4,32,2048]{2,1,0:T(8,128)(2,1)S(1)}, bf16[4,32,2048]{2,1,0:T(8,128)(2,1)}, u32[]{:S(2)}) copy-start(bf16[4,32,2048]{2,1,0:T(8,128)(2,1)} %param.21) | copy-start | bytes 1572868
  10.4 5.2 %copy-start.1 = (bf16[4,2048,256]{2,1,0:T(8,128)(2,1)S(1)}, bf16[4,2048,256]{2,1,0:T(8,128)(2,1)}, u32[]{:S(2)}) copy-start(bf16[4,2048,256]{2,1,0:T(8,128)(2,1)} %param.20) | copy-start | bytes 12582916
  14.1 2.3 %copy-start.9 = (bf16[4,256]{1,0:T(4,128)(2,1)}, bf16[4,256]{1,0:T(4,128)(2,1)S(1)}, u32[]{:S(2)}) copy-start(bf16[4,256]{1,0:T(4,128)(2,1)S(1)} %get-tuple-element.25) | copy-start | bytes 6148
  16.5 23.5 %copy-start.6 = (s32[64,2]{0,1:T(2,128)S(1)}, s32[64,2]{0,1:T(2,128)}, u32[]{:S(2)}) copy-start(s32[64,2]{0,1:T(2,128)} %param.34) | copy-start | bytes 1540
  16.8 24.0 %copy-start.8 = (bf16[2048]{0:T(1024)(128)(2,1)S(1)}, bf16[2048]{0:T(1024)(128)(2,1)}, u32[]{:S(2)}) copy-start(bf16[2048]{0:T(1024)(128)(2,1)} %param.31) | copy-start | bytes 12292
  17.6 17.3 %all-to-all-start = ((bf16[16,2,256]{2,1,0:T(2,128)(2,1)}), bf16[16,2,256]{2,1,0:T(2,128)(2,1)S(1)}, u32[]{:S(2)}, u32[]{:S(2)}) async-start(bf16[16,2,256]{2,1,0:T(2,128)(2,1)} %reshape.202), calls=%async_computation | async-start | bytes 32768 | tf_op jit(solution)/shard_map/all_to_all | solution.py:148
  28.9 44.6 %copy-start.11 = (bf16[2048,32]{0,1:T(8,128)(2,1)S(1)}, bf16[2048,32]{0,1:T(8,128)(2,1)}, u32[]{:S(2)}) copy-start(bf16[2048,32]{0,1:T(8,128)(2,1)} %param.33) | copy-start | bytes 393220
  35.1 38.7 %copy-start.12 = (bf16[2048,4]{0,1:T(4,128)(2,1)S(1)}, bf16[2048,4]{0,1:T(4,128)(2,1)}, u32[]{:S(2)}) copy-start(bf16[2048,4]{0,1:T(4,128)(2,1)} %param.32) | copy-start | bytes 49156
  36.2 21.1 %all-to-all-start.1 = ((f32[16,64,128]{2,1,0:T(8,128)}), f32[16,64,128]{2,1,0:T(8,128)S(1)}, u32[]{:S(2)}, u32[]{:S(2)}) async-start(f32[16,64,128]{2,1,0:T(8,128)} %convolution_bitcast_fusion), calls=%async_computation.1 | async-start | bytes 1048576 | tf_op jit(solution)/shard_map/all_to_all | solution.py:26
  73.7 24.1 %copy-start.2 = (bf16[2,2048,256]{2,1,0:T(8,128)(2,1)S(1)}, bf16[2,2048,256]{2,1,0:T(8,128)(2,1)}, u32[]{:S(2)}) copy-start(bf16[2,2048,256]{2,1,0:T(8,128)(2,1)} %param.35) | copy-start | bytes 6291460
  164.3 10.0 %all-to-all-start.4 = ((bf16[16,2,8,128]{3,2,1,0:T(8,128)(2,1)}), bf16[16,2,8,128]{3,2,1,0:T(8,128)(2,1)S(1)}, u32[]{:S(2)}, u32[]{:S(2)}) async-start(bf16[16,2,8,128]{3,2,1,0:T(8,128)(2,1)} %copy.106), calls=%async_computation.4 | async-start | bytes 131072 | tf_op jit(solution)/shard_map/all_to_all | solution.py:183
where the time goes:
time: 191 us; the launch traced here: 190 us
  blocking collectives  111 us (58%)
  waiting for transfers between devices  28.1 us (15%)
  starting transfers between devices  17.2 us (9%)
  matrix products  15.7 us (8%)
  other arithmetic  10 us (5%)
  local copies, waits for them, and re-layouts  7.45 us (4%)
    all_to_all x1, blocking collectives, sent_and_summed(): lax.all_to_all(tiles, axis, split_axis=0, concat_axis=0, tiled=True)  57.4 us
    all_to_all x1, blocking collectives, on_device(): lax.all_to_all(outbound, 'ep', split_axis=0, concat_axis=0, tiled=True)  23.1 us
    all_to_all x1, waiting for transfers between devices, sent_and_summed(): lax.all_to_all(tiles, axis, split_axis=0, concat_axis=0, tiled=True)  16.4 us
    all_gather x1, blocking collectives, on_device(): mixed = lax.all_gather(mixed_share, 'tp', axis=1, tiled=True)  15.4 us
    all_gather x1, blocking collectives, on_device(): after_attention = lax.all_gather(after_share, 'tp', axis=1, tiled=True)  15.2 us
    all_to_all x1, starting transfers between devices, on_device(): lax.all_to_all(head_values, 'tp', split_axis=1, concat_axis=0, tiled=True)  9.97 us
    all_to_all x1, waiting for transfers between devices, on_device(): lax.all_to_all(head_values, 'tp', split_axis=1, concat_axis=0, tiled=True)  6.01 us
    all_to_all x1, waiting for transfers between devices, on_device(): lax.all_to_all(summed_terms, 'ep', split_axis=0, concat_axis=0, tiled=True)  5.78 us
  transfers between devices with their start and end apart: 3, of which 3 were waited for; matrix products, arithmetic and copies ran while one was open for 2% of the time, Pallas kernels for 0%

commit v1 on v0

v1 whole, which is shorter than its diff:
```python
import functools
import math

import jax
import jax.numpy as jnp
from jax import lax
from jax.experimental import pallas as pl
from jax.experimental.pallas import tpu as pltpu
from jax.sharding import PartitionSpec as P

MESH = pl.DeviceIdType.MESH
F32 = jnp.float32
BF16 = jnp.bfloat16
I32 = jnp.int32

D = 2048
HALF = D // 2
H = 32
KV = 256
ROPE = 32
NOPE = 64
V = 64
GROUPS = 4
LEN = 2048
CAP = 8
N_EP = 16
N_TP = 16
NZ = 8
SEQS = 4
ROWS = 64
EXPERTS = 32
SLOTS = EXPERTS * CAP
SHARE = 128
HID = 256
EPS = 1e-06
ROPE_BASE = 10000.0


def dot(a, b):
    return jnp.dot(a, b, preferred_element_type=F32)


def dot_t(a, b):
    return lax.dot_general(a, b, (((1,), (1,)), ((), ())), preferred_element_type=F32)


def iota(shape, dim):
    return lax.broadcasted_iota(I32, shape, dim)


def kernel(
    residual,
    cache_latent,
    cache_rope,
    lengths,
    query_latent,
    query_rope,
    norm_gain,
    latent_weight,
    latent_gain,
    rope_weight,
    value_weight,
    out_weight,
    mixer_gain,
    group_router,
    expert_router,
    ids,
    gate_weight,
    up_weight,
    down_weight,
    mixed_out,
    new_latent_out,
    new_rope_out,
    res8,
    res_cols,
    cl,
    cr,
    ql,
    qr,
    ng,
    lw,
    lg,
    rw,
    vw,
    ow,
    mg,
    grt,
    ert,
    idv,
    gw,
    uw,
    dw,
    mixl,
    hv_send,
    hv_recv,
    acc,
    rs_send,
    rs_recv,
    after,
    after_other,
    full,
    sel,
    disp,
    xin,
    xn,
    ret,
    yin,
    comb,
    rs2_send,
    rs2_recv,
    fin,
    local_sem,
    w_ssem,
    w_rsem,
    hv_ssem,
    hv_rsem,
    rs_ssem,
    rs_rsem,
    ag_ssem,
    ag_rsem,
    ot_ssem,
    ot_rsem,
    x_ssem,
    x_rsem,
    y_ssem,
    y_rsem,
    rs2_ssem,
    rs2_rsem,
    f_ssem,
    f_rsem,
    p_ssem,
    p_rsem,
):
    ep = lax.axis_index("ep")
    tp = lax.axis_index("tp")
    z = lax.div(tp, 2)
    c = lax.rem(tp, 2)
    other = 1 - c
    partner = z * 2 + other

    def remote(src, dst, ssem, rsem, to_ep, to_tp):
        return pltpu.make_async_remote_copy(
            src_ref=src,
            dst_ref=dst,
            send_sem=ssem,
            recv_sem=rsem,
            device_id=(to_ep, to_tp),
            device_id_type=MESH,
        )

    def ring(i):
        return lax.rem(z + i, NZ)

    barrier = pltpu.get_barrier_semaphore()

    def signal_tp(i, carry):
        pl.semaphore_signal(
            barrier, inc=1, device_id=(ep, lax.rem(tp + i, N_TP)), device_id_type=MESH
        )
        return carry

    def signal_ep(i, carry):
        there = lax.rem(ep + i, N_EP)
        for core in range(2):
            pl.semaphore_signal(
                barrier, inc=1, device_id=(there, z * 2 + core), device_id_type=MESH
            )
        return carry

    lax.fori_loop(1, N_TP, signal_tp, 0)
    lax.fori_loop(1, N_EP, signal_ep, 0)

    loads = {}

    def load(name, src, dst):
        copy = pltpu.make_async_copy(src, dst, local_sem.at[len(loads)])
        copy.start()
        loads[name] = copy

    load("res8", residual.at[pl.ds(pl.multiple_of(z * 8, 8), 8), :], res8)
    load("ng", norm_gain, ng)
    load("lg", latent_gain, lg)
    load("rw", rope_weight, rw)
    load("qr", query_rope, qr)
    load("lw", latent_weight, lw)
    load("ql", query_latent, ql)
    for s in range(SEQS):
        load(f"cr{s}", cache_rope.at[s], cr.at[s])
        load(f"cl{s}", cache_latent.at[s], cl.at[s])
    load("vw", value_weight, vw)
    load("ow", out_weight.at[:, pl.ds(pl.multiple_of(c * HALF, HALF), HALF)], ow.at[c])
    share_at = pl.multiple_of(c * HALF + z * SHARE, SHARE)
    load("res_cols", residual.at[:, pl.ds(share_at, SHARE)], res_cols)
    load("ids", ids, idv)
    load("mg", mixer_gain, mg)
    load("grt", group_router, grt)
    load("ert", expert_router, ert)
    load("gw", gate_weight.at[c], gw.at[0])
    load("uw", up_weight.at[c], uw.at[0])
    load("dw", down_weight.at[c], dw.at[0])

    loads["res8"].wait()
    loads["ng"].wait()
    rows = res8[...].astype(F32)
    inv = lax.rsqrt(jnp.mean(rows * rows, axis=1, keepdims=True) + EPS)
    normed = (rows * inv * ng[...].astype(F32)).astype(BF16)
    loads["rw"].wait()
    rope_raw = dot_t(normed, rw[...])
    loads["lw"].wait()
    latent_raw = dot(normed, lw[...])
    inv = lax.rsqrt(jnp.mean(latent_raw * latent_raw, axis=1, keepdims=True) + EPS)
    loads["lg"].wait()
    latent8 = latent_raw * inv * lg[...].astype(F32)

    def own_rows(v):
        first = (iota(v.shape, 0) * 0 + c) == 0
        return jnp.where(first, v, pltpu.roll(v, 4, 0))

    new_latent = own_rows(latent8).astype(BF16)
    new_latent_out[...] = new_latent[0:SEQS]
    rope_own = own_rows(rope_raw)

    lane = iota((8, ROPE), 1)
    row = iota((8, ROPE), 0)
    place = lax.rem(lane, ROPE // 2).astype(F32)
    freq = jnp.exp(place * (-math.log(ROPE_BASE) / (ROPE // 2)))
    pos = jnp.zeros((8, ROPE), I32)
    for s in range(SEQS):
        pos = jnp.where(row == s, lengths[s], pos)
    angle = pos.astype(F32) * freq
    cos = jnp.cos(angle)
    sin = jnp.sin(angle)
    sin = jnp.where(lane < ROPE // 2, -sin, sin)

    def swapped(u):
        return jnp.concatenate([u[:, ROPE // 2 :], u[:, : ROPE // 2]], axis=1)

    new_rope = (rope_own * cos + swapped(rope_own) * sin).astype(BF16)
    new_rope_out[...] = new_rope[0:SEQS]
    new_latent_f = new_latent.astype(F32)
    new_rope_f = new_rope.astype(F32)

    scale = (NOPE + ROPE) ** (-0.5)
    loads["qr"].wait()
    loads["ql"].wait()
    for s in range(SEQS):
        u = qr[s].astype(F32)
        turned = (u * cos[s : s + 1] + swapped(u) * sin[s : s + 1]).astype(BF16)
        q = ql[s]
        loads[f"cr{s}"].wait()
        loads[f"cl{s}"].wait()
        latents = cl[s]
        score = (dot_t(q, latents) + dot(turned, cr[s])) * scale
        keep = iota((H, LEN), 1) < lengths[s]
        score = jnp.where(keep, score, -jnp.inf)
        fresh = (
            jnp.sum(q.astype(F32) * new_latent_f[s : s + 1], axis=1, keepdims=True)
            + jnp.sum(turned.astype(F32) * new_rope_f[s : s + 1], axis=1, keepdims=True)
        ) * scale
        top = jnp.maximum(jnp.max(score, axis=1, keepdims=True), fresh)
        e = jnp.exp(score - top)
        fresh_e = jnp.exp(fresh - top)
        total = jnp.sum(e, axis=1, keepdims=True) + fresh_e
        weight = (e / total).astype(BF16)
        fresh_w = (fresh_e / total).astype(BF16).astype(F32)
        mixed = dot(weight, latents) + fresh_w * new_latent_f[s : s + 1]
        mixl[s * H : (s + 1) * H, :] = mixed.astype(BF16)
        if s == 0:
            pl.semaphore_wait(barrier, 45)
            swaps = [
                remote(
                    out_weight.at[:, pl.ds(pl.multiple_of(other * HALF, HALF), HALF)],
                    ow.at[c],
                    w_ssem.at[0],
                    w_rsem.at[0],
                    ep,
                    partner,
                ),
                remote(gate_weight.at[other], gw.at[1], w_ssem.at[1], w_rsem.at[1], ep, partner),
                remote(up_weight.at[other], uw.at[1], w_ssem.at[2], w_rsem.at[2], ep, partner),
                remote(down_weight.at[other], dw.at[1], w_ssem.at[3], w_rsem.at[3], ep, partner),
            ]
            for copy in swaps:
                copy.start()

    loads["vw"].wait()
    wide = dot(mixl[...], vw[...])
    own = (iota((SEQS * H, D), 1) // V) == lax.rem(iota((SEQS * H, D), 0), H)
    wide = jnp.where(own, wide, 0.0).astype(BF16)
    pick = (iota((8, SEQS * H), 1) // H) == lax.rem(iota((8, SEQS * H), 0), SEQS)
    heads = dot(pick.astype(F32).astype(BF16), wide)
    low = iota((8, SHARE), 0) < SEQS
    for zz in range(NZ):
        a = heads[:, zz * 256 : zz * 256 + 128]
        b = heads[:, zz * 256 + 128 : zz * 256 + 256]
        hv_send[zz] = jnp.where(low, a, b).astype(BF16)

    def hv_copy(i):
        there = lax.rem(tp + i, N_TP)
        return remote(
            hv_send.at[lax.div(there, 2)], hv_recv.at[tp], hv_ssem.at[i], hv_rsem.at[tp], ep, there
        )

    def hv_start(i, carry):
        hv_copy(lax.rem(i + 7, N_TP - 1) + 1).start()
        return carry

    lax.fori_loop(0, N_TP - 1, hv_start, 0)
    hv_recv[tp] = hv_send[z]

    loads["ids"].wait()
    idr = idv[...]
    e_row = [idr[k : k + 1, :] for k in range(2)]
    eye = iota((ROWS, ROWS), 0) == iota((ROWS, ROWS), 1)

    def to_col(v):
        return jnp.sum(jnp.where(eye, jnp.broadcast_to(v, (ROWS, ROWS)), 0.0), axis=1, keepdims=True)

    def to_row(v):
        return jnp.sum(jnp.where(eye, jnp.broadcast_to(v, (ROWS, ROWS)), 0.0), axis=0, keepdims=True)

    e_col = [to_col(v.astype(F32)) for v in e_row]
    expert_iota = iota((ROWS, EXPERTS), 1).astype(F32)
    hits = [(jnp.broadcast_to(v, (ROWS, EXPERTS)) == expert_iota).astype(F32) for v in e_col]
    before = (iota((ROWS, ROWS), 1) < iota((ROWS, ROWS), 0)).astype(F32).astype(BF16)
    counts = dot(before, (hits[0] + hits[1]).astype(BF16))
    slot_col = [
        e_col[k] * CAP + jnp.sum(counts * hits[k], axis=1, keepdims=True) for k in range(2)
    ]
    slot_iota = iota((SLOTS, ROWS), 0).astype(F32)
    chosen = jnp.zeros((SLOTS, ROWS), F32)
    for k in range(2):
        chosen += (jnp.broadcast_to(to_row(slot_col[k]), (SLOTS, ROWS)) == slot_iota).astype(F32)
    sel[...] = chosen.astype(BF16)

    def hv_wait(i, carry):
        src = lax.rem(tp + i, N_TP)
        remote(
            hv_send.at[0], hv_recv.at[src], hv_ssem.at[i], hv_rsem.at[src], ep, src
        ).wait_recv()
        return carry

    lax.fori_loop(1, N_TP, hv_wait, 0)

    loads["ow"].wait()
    swaps[0].wait_recv()
    heads_in = hv_recv[...].astype(F32).reshape(N_TP * 8, SHARE).astype(BF16)
    part = None
    for k in range(2):
        r = iota((ROWS, N_TP * 8), 0)
        j = iota((ROWS, N_TP * 8), 1)
        rows_k = (j == 8 * (r // SEQS) + SEQS * k + lax.rem(r, SEQS)).astype(F32).astype(BF16)
        term = dot(dot(rows_k, heads_in).astype(BF16), ow[k])
        part = term if part is None else part + term
    for zz in range(NZ):
        piece = part[:, zz * SHARE : (zz + 1) * SHARE]
        acc[zz] = piece
        rs_send[zz] = piece.astype(BF16)

    order = (4, 3, 5, 2, 6, 1, 7)

    def scatter(send, recv, ssem, rsem):
        def copy(i):
            to = ring(i)
            return remote(
                send.at[to], recv.at[z], ssem.at[i], rsem.at[z], ep, to * 2 + c
            )

        for i in order:
            copy(i).start()

    def scatter_wait(send, recv, ssem, rsem, total):
        for i in reversed(order):
            src = ring(i)
            remote(
                send.at[src], recv.at[src], ssem.at[i], rsem.at[src], ep, src * 2 + c
            ).wait_recv()
            total += recv[src].astype(F32)
        return total

    scatter(rs_send, rs_recv, rs_ssem, rs_rsem)
    loads["res_cols"].wait()
    total = res_cols[...].astype(F32) + scatter_wait(rs_send, rs_recv, rs_ssem, rs_rsem, acc[z])
    after[z] = total.astype(BF16)

    def ag_copy(i, src):
        return remote(
            after.at[src], after.at[src], ag_ssem.at[i], ag_rsem.at[src], ep, ring(i) * 2 + c
        )

    for i in order:
        ag_copy(i, z).start()

    def place_slots(zz):
        at = pl.ds(pl.multiple_of(zz * SHARE, SHARE), SHARE)
        disp[:, at] = dot(sel[...], after[zz]).astype(BF16)

    place_slots(z)
    for i in reversed(order):
        src = ring(i)
        remote(
            after.at[z], after.at[src], ag_ssem.at[i], ag_rsem.at[src], ep, src * 2 + c
        ).wait_recv()
        place_slots(src)

    def x_copy(i, core):
        there = lax.rem(ep + i, N_EP)
        at = pl.ds(pl.multiple_of((there * 2 + core) * CAP, CAP), CAP)
        to = pl.ds(pl.multiple_of(ep * CAP, CAP), CAP)
        return remote(
            disp.at[at, :],
            xin.at[c, to, :],
            x_ssem.at[i * 2 + core],
            x_rsem.at[ep * 2 + c],
            there,
            z * 2 + core,
        )

    def x_start(i, carry):
        for core in range(2):
            x_copy(i, core).start()
        return carry

    lax.fori_loop(1, N_EP, x_start, 0)
    x_copy(0, other).start()
    mine = pl.ds(pl.multiple_of((ep * 2 + c) * CAP, CAP), CAP)
    here = pl.ds(pl.multiple_of(ep * CAP, CAP), CAP)
    xin[c, here, :] = disp[mine, :]
    to_partner = remote(after, after_other, ot_ssem, ot_rsem, ep, partner)
    to_partner.start()

    loads["mg"].wait()
    loads["grt"].wait()
    loads["ert"].wait()
    to_partner.wait_recv()
    for zz in range(NZ):
        at = pl.ds(pl.multiple_of(c * HALF + zz * SHARE, SHARE), SHARE)
        full[:, at] = after[zz]
        at = pl.ds(pl.multiple_of(other * HALF + zz * SHARE, SHARE), SHARE)
        full[:, at] = after_other[zz]
    gain = mg[...].astype(F32)
    rows = full[...].astype(F32)
    inv = lax.rsqrt(jnp.mean(rows * rows, axis=1, keepdims=True) + EPS)
    expert_in = (rows * inv * gain).astype(BF16)
    group_logits = dot_t(expert_in, grt[...])
    expert_logits = dot_t(expert_in, ert[...])
    group_of = jnp.floor(e_col[0] * (GROUPS / EXPERTS))
    group_hit = jnp.broadcast_to(group_of, (ROWS, GROUPS)) == iota((ROWS, GROUPS), 1).astype(F32)
    group_pick = jnp.sum(jnp.where(group_hit, group_logits, 0.0), axis=1, keepdims=True)
    share = 1.0 / jnp.sum(jnp.exp(group_logits - group_pick), axis=1, keepdims=True)
    picked = [jnp.sum(hits[k] * expert_logits, axis=1, keepdims=True) for k in range(2)]
    weights = jnp.zeros((ROWS, SLOTS), F32)
    wide_iota = iota((ROWS, SLOTS), 1).astype(F32)
    for k in range(2):
        inner = 1.0 / (1.0 + jnp.exp(picked[1 - k] - picked[k]))
        weights += jnp.where(
            jnp.broadcast_to(slot_col[k], (ROWS, SLOTS)) == wide_iota, share * inner, 0.0
        )
    high = weights.astype(BF16)
    comb[0:ROWS, :] = high
    comb[ROWS:, :] = (weights - high.astype(F32)).astype(BF16)

    def x_wait(i, carry):
        src = lax.rem(ep + i, N_EP)
        at = pl.ds(pl.multiple_of(src * CAP, CAP), CAP)
        for core in range(2):
            remote(
                disp.at[at, :],
                xin.at[core, at, :],
                x_ssem.at[i * 2 + core],
                x_rsem.at[src * 2 + core],
                src,
                z * 2 + core,
            ).wait_recv()
        return carry

    remote(
        disp.at[here, :],
        xin.at[other, here, :],
        x_ssem.at[other],
        x_rsem.at[ep * 2 + other],
        ep,
        partner,
    ).wait_recv()
    lax.fori_loop(1, N_EP, x_wait, 0)
    x0 = xin[0].astype(F32)
    x1 = xin[1].astype(F32)
    square = jnp.sum(x0 * x0, axis=1, keepdims=True) + jnp.sum(x1 * x1, axis=1, keepdims=True)
    inv = lax.rsqrt(square * (1.0 / D) + EPS)
    xn[:, 0:HALF] = (x0 * inv * gain[:, 0:HALF]).astype(BF16)
    xn[:, HALF:] = (x1 * inv * gain[:, HALF:]).astype(BF16)
    acts = []
    for name in ("gw", "uw", "dw"):
        loads[name].wait()
    for copy in swaps[1:]:
        copy.wait_recv()
    for k in range(2):
        g = dot(xn[...], gw[k])
        u = dot(xn[...], uw[k])
        acts.append((g * (1.0 / (1.0 + jnp.exp(-g))) * u).astype(BF16))

    def y_copy(i, half):
        there = lax.rem(ep + i, N_EP)
        at = pl.ds(pl.multiple_of(there * CAP, CAP), CAP)
        return remote(
            ret.at[half, at, :],
            yin.at[mine, :],
            y_ssem.at[i * 2 + half],
            y_rsem.at[ep * 2 + c],
            there,
            z * 2 + half,
        )

    for half in range(2):
        cols = slice(half * HALF, (half + 1) * HALF)
        ret[half] = (dot(acts[0], dw[0, :, cols]) + dot(acts[1], dw[1, :, cols])).astype(BF16)

        def y_start(i, carry, half=half):
            y_copy(i, half).start()
            return carry

        lax.fori_loop(1, N_EP, y_start, 0)
    y_copy(0, other).start()
    yin[mine, :] = ret[c, here, :]

    def y_wait(i, carry):
        src = lax.rem(ep + i, N_EP)
        for core in range(2):
            at = pl.ds(pl.multiple_of((src * 2 + core) * CAP, CAP), CAP)
            remote(
                ret.at[core, here, :],
                yin.at[at, :],
                y_ssem.at[i * 2 + core],
                y_rsem.at[src * 2 + core],
                src,
                z * 2 + core,
            ).wait_recv()
        return carry

    theirs = pl.ds(pl.multiple_of((ep * 2 + other) * CAP, CAP), CAP)
    remote(
        ret.at[other, here, :],
        yin.at[theirs, :],
        y_ssem.at[other],
        y_rsem.at[ep * 2 + other],
        ep,
        partner,
    ).wait_recv()
    lax.fori_loop(1, N_EP, y_wait, 0)

    both = dot(comb[...], yin[...])
    moe = both[0:ROWS] + both[ROWS:]
    for zz in range(NZ):
        piece = moe[:, zz * SHARE : (zz + 1) * SHARE]
        acc[zz] = piece
        rs2_send[zz] = piece.astype(BF16)
    scatter(rs2_send, rs2_recv, rs2_ssem, rs2_rsem)
    total = after[z].astype(F32) + scatter_wait(rs2_send, rs2_recv, rs2_ssem, rs2_rsem, acc[z])
    fin[c, z] = total.astype(BF16)

    def f_copy(i):
        return remote(
            fin.at[c, z], fin.at[c, z], f_ssem.at[i], f_rsem.at[z], ep, ring(i) * 2 + c
        )

    def p_copy(zz, i):
        return remote(fin.at[c, zz], fin.at[c, zz], p_ssem.at[i], p_rsem.at[zz], ep, partner)

    for i in order:
        f_copy(i).start()
    p_copy(z, 0).start()
    for i in reversed(order):
        src = ring(i)
        remote(
            fin.at[c, src], fin.at[c, src], f_ssem.at[i], f_rsem.at[src], ep, src * 2 + c
        ).wait_recv()
        p_copy(src, i).start()

    def spread(core, zz):
        at = pl.ds(pl.multiple_of(core * HALF + zz * SHARE, SHARE), SHARE)
        mixed_out[:, at] = fin[core, zz]

    for zz in range(NZ):
        spread(c, zz)
    for i in (0,) + order[::-1]:
        src = ring(i)
        remote(
            fin.at[other, src], fin.at[other, src], p_ssem.at[i], p_rsem.at[src], ep, partner
        ).wait_recv()
        spread(other, src)

    for copy in swaps:
        copy.wait_send()

    def hv_drain(i, carry):
        hv_copy(i).wait_send()
        return carry

    lax.fori_loop(1, N_TP, hv_drain, 0)
    for i in order:
        to = ring(i)
        remote(rs_send.at[to], rs_recv.at[z], rs_ssem.at[i], rs_rsem.at[z], ep, to * 2 + c).wait_send()
        ag_copy(i, z).wait_send()
        remote(
            rs2_send.at[to], rs2_recv.at[z], rs2_ssem.at[i], rs2_rsem.at[z], ep, to * 2 + c
        ).wait_send()
        f_copy(i).wait_send()
        p_copy(ring(i), i).wait_send()
    p_copy(z, 0).wait_send()
    to_partner.wait_send()
    x_copy(0, other).wait_send()
    y_copy(0, other).wait_send()

    def xy_drain(i, carry):
        for core in range(2):
            x_copy(i, core).wait_send()
            y_copy(i, core).wait_send()
        return carry

    lax.fori_loop(1, N_EP, xy_drain, 0)


def on_device(
    residual,
    cache_latent,
    cache_rope,
    lengths,
    query_latent,
    query_rope,
    norm_gain,
    latent_weight,
    latent_gain,
    rope_weight,
    value_weight,
    out_weight,
    mixer_gain,
    group_router,
    expert_router,
    expert_ids,
    gate_weight,
    up_weight,
    down_weight,
):
    anywhere = pl.BlockSpec(memory_space=pl.ANY)
    vmem = pl.BlockSpec(memory_space=pltpu.VMEM)
    smem = pl.BlockSpec(memory_space=pltpu.SMEM)
    dma = pltpu.SemaphoreType.DMA
    in_specs = [anywhere] * 19
    in_specs[3] = smem
    return pl.pallas_call(
        kernel,
        out_shape=(
            jax.ShapeDtypeStruct((ROWS, D), BF16),
            jax.ShapeDtypeStruct((SEQS, KV), BF16),
            jax.ShapeDtypeStruct((SEQS, ROPE), BF16),
        ),
        in_specs=in_specs,
        out_specs=(vmem, vmem, vmem),
        scratch_shapes=[
            pltpu.VMEM((8, D), BF16),
            pltpu.VMEM((ROWS, SHARE), BF16),
            pltpu.VMEM((SEQS, LEN, KV), BF16),
            pltpu.VMEM((SEQS, ROPE, LEN), BF16),
            pltpu.VMEM((SEQS, H, KV), BF16),
            pltpu.VMEM((SEQS, H, ROPE), BF16),
            pltpu.VMEM((1, D), BF16),
            pltpu.VMEM((D, KV), BF16),
            pltpu.VMEM((1, KV), BF16),
            pltpu.VMEM((ROPE, D), BF16),
            pltpu.VMEM((KV, D), BF16),
            pltpu.VMEM((2, SHARE, HALF), BF16),
            pltpu.VMEM((1, D), BF16),
            pltpu.VMEM((GROUPS, D), BF16),
            pltpu.VMEM((EXPERTS, D), BF16),
            pltpu.VMEM((2, ROWS), I32),
            pltpu.VMEM((2, D, HID), BF16),
            pltpu.VMEM((2, D, HID), BF16),
            pltpu.VMEM((2, HID, D), BF16),
            pltpu.VMEM((SEQS * H, KV), BF16),
            pltpu.VMEM((NZ, 8, SHARE), BF16),
            pltpu.VMEM((N_TP, 8, SHARE), BF16),
            pltpu.VMEM((NZ, ROWS, SHARE), F32),
            pltpu.VMEM((NZ, ROWS, SHARE), BF16),
            pltpu.VMEM((NZ, ROWS, SHARE), BF16),
            pltpu.VMEM((NZ, ROWS, SHARE), BF16),
            pltpu.VMEM((NZ, ROWS, SHARE), BF16),
            pltpu.VMEM((ROWS, D), BF16),
            pltpu.VMEM((SLOTS, ROWS), BF16),
            pltpu.VMEM((SLOTS, HALF), BF16),
            pltpu.VMEM((2, N_EP * CAP, HALF), BF16),
            pltpu.VMEM((N_EP * CAP, D), BF16),
            pltpu.VMEM((2, N_EP * CAP, HALF), BF16),
            pltpu.VMEM((SLOTS, HALF), BF16),
            pltpu.VMEM((2 * ROWS, SLOTS), BF16),
            pltpu.VMEM((NZ, ROWS, SHARE), BF16),
            pltpu.VMEM((NZ, ROWS, SHARE), BF16),
            pltpu.VMEM((2, NZ, ROWS, SHARE), BF16),
            dma((32,)),
            dma((4,)),
            dma((4,)),
            dma((N_TP,)),
            dma((N_TP,)),
            dma((NZ,)),
            dma((NZ,)),
            dma((NZ,)),
            dma((NZ,)),
            dma,
            dma,
            dma((2 * N_EP,)),
            dma((2 * N_EP,)),
            dma((2 * N_EP,)),
            dma((2 * N_EP,)),
            dma((NZ,)),
            dma((NZ,)),
            dma((NZ,)),
            dma((NZ,)),
            dma((NZ,)),
            dma((NZ,)),
        ],
        compiler_params=pltpu.CompilerParams(
            collective_id=0, has_side_effects=True, vmem_limit_bytes=60 * 1024 * 1024
        ),
    )(
        residual,
        cache_latent,
        cache_rope,
        lengths,
        query_latent,
        query_rope,
        norm_gain.reshape(1, D),
        latent_weight,
        latent_gain.reshape(1, KV),
        rope_weight,
        value_weight,
        out_weight,
        mixer_gain.reshape(1, D),
        group_router.T,
        expert_router.T,
        expert_ids.T,
        gate_weight,
        up_weight,
        down_weight,
    )


def solution(mesh):
    in_specs = (
        P("ep", None),
        P(("ep", "tp"), None, None),
        P(("ep", "tp"), None, None),
        P(("ep", "tp")),
        P(("ep", "tp"), None, None),
        P(("ep", "tp"), None, None),
        P(),
        P(),
        P(),
        P(),
        P(),
        P("tp", None),
        P(),
        P(),
        P(),
        P("ep", None),
        P("ep", None, "tp"),
        P("ep", None, "tp"),
        P("ep", "tp", None),
    )
    out_specs = (P("ep", None), P(("ep", "tp"), None), P(("ep", "tp"), None))
    return jax.shard_map(
        on_device, mesh=mesh, in_specs=in_specs, out_specs=out_specs, check_vma=False
    )
```

time: 191 us -> 71.3 us (0.37)
  blocking collectives: 111 us -> 0 us
  Pallas kernels: 0 us -> 62.3 us
  waiting for transfers between devices: 28.1 us -> 0 us
  starting transfers between devices: 17.2 us -> 0 us
  matrix products: 15.7 us -> 0 us
  other arithmetic: 10 us -> 0 us
    all_to_all x2 -> x0, blocking collectives: 80.4 us -> none  [the longest x1 57.4 us: sent_and_summed(): lax.all_to_all(tiles, axis, split_axis=0, concat_axis=0, tiled=True)]
    pallas_call x0 -> x1, Pallas kernels: none -> 62.3 us  [on_device(): pl.pallas_call(kernel, out_shape=(jax.ShapeDtypeStruct((ROWS, D), BF16),...]
    all_gather x2 -> x0, blocking collectives: 30.5 us -> none  [the longest x1 15.4 us: on_device(): mixed = lax.all_gather(mixed_share, 'tp', axis=1, tiled=True)]
    all_to_all x3 -> x0, waiting for transfers between devices: 28.1 us -> none  [the longest x1 16.4 us: sent_and_summed(): lax.all_to_all(tiles, axis, split_axis=0, concat_axis=0, tiled=True)]
    all_to_all x3 -> x0, starting transfers between devices: 17.2 us -> none  [the longest x1 9.97 us: on_device(): lax.all_to_all(head_values, 'tp', split_axis=1, concat_axis=0, tiled=True)]
    dot_general x15 -> x0, matrix products: 15.7 us -> none  [the longest x1 3.79 us: on_device(): jnp.einsum('secf,efd->secd', activation, down_weight, preferred_element_t...]
    convert_element_type x11 -> x0, other arithmetic: 4.57 us -> none  [the longest x1 1.32 us: on_device(): positions = lengths.astype(jnp.float32)]
    reduce_sum x10 -> x0, other arithmetic: 3.54 us -> none  [the longest x2 1.73 us: sent_and_summed(): return arrived.sum(axis=0)]
  transfers between devices with their start and end apart: 3 -> 0, of which waited for: 3 -> 0; matrix products, arithmetic and copies ran while one was open for 2% -> 0% of each run, Pallas kernels for 0% -> 0%
where the time goes in v1:
time: 71.3 us; the launch traced here: 70.9 us
  Pallas kernels  62.3 us (87%)
  local copies, waits for them, and re-layouts  7.97 us (11%)
    pallas_call x1, Pallas kernels, on_device(): pl.pallas_call(kernel, out_shape=(jax.ShapeDtypeStruct((ROWS, D), BF16),...  62.3 us
    unnamed x3, local copies, waits for them, and re-layouts  4.17 us

profile of v1, /device:TPU:1, one launch (start us, length us, event | category | flops | bytes accessed | tf_op | source)
XLA Modules:
  0.0 70.9 jit_solution(8123282658762711409)
XLA Ops:
  0.6 1.2 %reshape.16.latent_gain = bf16[1,256]{1,0:T(2,128)(2,1)} reshape(bf16[256]{0:T(256)(128)(2,1)} %param.27) | data formatting | bytes 1024 | tf_op jit(solution)/shard_map/reshape | solution.py:732
  1.9 1.3 %reshape.15.norm_gain = bf16[1,2048]{1,0:T(2,128)(2,1)} reshape(bf16[2048]{0:T(1024)(128)(2,1)} %param.25) | data formatting | bytes 8192 | tf_op jit(solution)/shard_map/reshape | solution.py:730
  3.1 1.3 %reshape.17.mixer_gain = bf16[1,2048]{1,0:T(2,128)(2,1)} reshape(bf16[2048]{0:T(1024)(128)(2,1)} %param.31) | data formatting | bytes 8192 | tf_op jit(solution)/shard_map/reshape | solution.py:736
  4.4 62.3 %shard_map.202 = (bf16[64,2048]{1,0:T(8,128)(2,1)}, bf16[4,256]{1,0:T(4,128)(2,1)}, bf16[4,32]{1,0:T(4,128)(2,1)}) custom-call(bf16[64,2048]{1,0:T(8,128)(2,1)} %residual.1, bf16[4,2048,256]{2,1,0:T(8,128)(2,1)} %cache_latent.1, bf16[4,32,2048]{2,1,0:T(8,128)(2,1)} %cache_rope.1, s32[4]{0:T(128)} %lengths.1, bf16[4,32,256]{2,1,0:T(8,128)(2,1)} %query_latent.1, ...), custom_call_target="tpu_custom_call" | custom-call | tf_op jit(solution)/shard_map/pallas_call | solution.py:650
  66.7 1.7 %copy.25 = bf16[64,2048]{1,0:T(8,128)(2,1)} copy(bf16[64,2048]{1,0:T(8,128)(2,1)} %get-tuple-element.6) | data formatting | bytes 524288
  68.4 1.3 %copy.26 = bf16[4,256]{1,0:T(4,128)(2,1)} copy(bf16[4,256]{1,0:T(4,128)(2,1)} %get-tuple-element.7) | data formatting | bytes 4096
  69.6 1.2 %copy.27 = bf16[4,32]{1,0:T(4,128)(2,1)} copy(bf16[4,32]{1,0:T(4,128)(2,1)} %get-tuple-element.8) | data formatting | bytes 512

commit v2 on v1

--- a/solution.py
+++ b/solution.py
@@ -32,8 +32,20 @@
 SLOTS = EXPERTS * CAP
 SHARE = 128
 HID = 256
+OTHERS = 2 * N_EP - 1
 EPS = 1e-06
 ROPE_BASE = 10000.0
+ORDER = (4, 3, 5, 2, 6, 1, 7)
+OUT_GROUPS = ((0, 1, 7), (2, 6), (3, 5, 4))
+BACK_GROUPS = ((4, 3, 5, 2), (6, 1, 7, 0))
+
+
+def spans(groups):
+    at, result = 0, []
+    for group in groups:
+        result.append((at * SHARE, len(group) * SHARE))
+        at += len(group)
+    return result
 
 
 def dot(a, b):
@@ -52,7 +64,7 @@
     residual,
     cache_latent,
     cache_rope,
-    lengths,
+    lengths_in,
     query_latent,
     query_rope,
     norm_gain,
@@ -71,6 +83,7 @@
     mixed_out,
     new_latent_out,
     new_rope_out,
+    lengths,
     res8,
     res_cols,
     cl,
@@ -109,6 +122,8 @@
     rs2_send,
     rs2_recv,
     fin,
+    gain2,
+    lt,
     local_sem,
     w_ssem,
     w_rsem,
@@ -167,9 +182,6 @@
             )
         return carry
 
-    lax.fori_loop(1, N_TP, signal_tp, 0)
-    lax.fori_loop(1, N_EP, signal_ep, 0)
-
     loads = {}
 
     def load(name, src, dst):
@@ -177,6 +189,7 @@
         copy.start()
         loads[name] = copy
 
+    load("len", lengths_in, lengths)
     load("res8", residual.at[pl.ds(pl.multiple_of(z * 8, 8), 8), :], res8)
     load("ng", norm_gain, ng)
     load("lg", latent_gain, lg)
@@ -187,30 +200,22 @@
     for s in range(SEQS):
         load(f"cr{s}", cache_rope.at[s], cr.at[s])
         load(f"cl{s}", cache_latent.at[s], cl.at[s])
-    load("vw", value_weight, vw)
-    load("ow", out_weight.at[:, pl.ds(pl.multiple_of(c * HALF, HALF), HALF)], ow.at[c])
-    share_at = pl.multiple_of(c * HALF + z * SHARE, SHARE)
-    load("res_cols", residual.at[:, pl.ds(share_at, SHARE)], res_cols)
-    load("ids", ids, idv)
-    load("mg", mixer_gain, mg)
-    load("grt", group_router, grt)
-    load("ert", expert_router, ert)
-    load("gw", gate_weight.at[c], gw.at[0])
-    load("uw", up_weight.at[c], uw.at[0])
-    load("dw", down_weight.at[c], dw.at[0])
+
+    lax.fori_loop(1, N_TP, signal_tp, 0)
+    lax.fori_loop(1, N_EP, signal_ep, 0)
 
     loads["res8"].wait()
     loads["ng"].wait()
     rows = res8[...].astype(F32)
     inv = lax.rsqrt(jnp.mean(rows * rows, axis=1, keepdims=True) + EPS)
-    normed = (rows * inv * ng[...].astype(F32)).astype(BF16)
+    normed = (rows * inv * ng[...].astype(F32)[None, :]).astype(BF16)
     loads["rw"].wait()
     rope_raw = dot_t(normed, rw[...])
     loads["lw"].wait()
     latent_raw = dot(normed, lw[...])
     inv = lax.rsqrt(jnp.mean(latent_raw * latent_raw, axis=1, keepdims=True) + EPS)
     loads["lg"].wait()
-    latent8 = latent_raw * inv * lg[...].astype(F32)
+    latent8 = latent_raw * inv * lg[...].astype(F32)[None, :]
 
     def own_rows(v):
         first = (iota(v.shape, 0) * 0 + c) == 0
@@ -220,6 +225,7 @@
     new_latent_out[...] = new_latent[0:SEQS]
     rope_own = own_rows(rope_raw)
 
+    loads["len"].wait()
     lane = iota((8, ROPE), 1)
     row = iota((8, ROPE), 0)
     place = lax.rem(lane, ROPE // 2).astype(F32)
@@ -243,14 +249,13 @@
     scale = (NOPE + ROPE) ** (-0.5)
     loads["qr"].wait()
     loads["ql"].wait()
-    for s in range(SEQS):
+    def attend(s):
         u = qr[s].astype(F32)
         turned = (u * cos[s : s + 1] + swapped(u) * sin[s : s + 1]).astype(BF16)
         q = ql[s]
-        loads[f"cr{s}"].wait()
-        loads[f"cl{s}"].wait()
         latents = cl[s]
-        score = (dot_t(q, latents) + dot(turned, cr[s])) * scale
+        lt[s] = latents.T
+        score = (dot(q, lt[s]) + dot(turned, cr[s])) * scale
         keep = iota((H, LEN), 1) < lengths[s]
         score = jnp.where(keep, score, -jnp.inf)
         fresh = (
@@ -265,23 +270,37 @@
         fresh_w = (fresh_e / total).astype(BF16).astype(F32)
         mixed = dot(weight, latents) + fresh_w * new_latent_f[s : s + 1]
         mixl[s * H : (s + 1) * H, :] = mixed.astype(BF16)
-        if s == 0:
-            pl.semaphore_wait(barrier, 45)
-            swaps = [
-                remote(
-                    out_weight.at[:, pl.ds(pl.multiple_of(other * HALF, HALF), HALF)],
-                    ow.at[c],
-                    w_ssem.at[0],
-                    w_rsem.at[0],
-                    ep,
-                    partner,
-                ),
-                remote(gate_weight.at[other], gw.at[1], w_ssem.at[1], w_rsem.at[1], ep, partner),
-                remote(up_weight.at[other], uw.at[1], w_ssem.at[2], w_rsem.at[2], ep, partner),
-                remote(down_weight.at[other], dw.at[1], w_ssem.at[3], w_rsem.at[3], ep, partner),
-            ]
-            for copy in swaps:
-                copy.start()
+
+    for pair in range(0, SEQS, 2):
+        for s in range(pair, pair + 2):
+            loads[f"cr{s}"].wait()
+            loads[f"cl{s}"].wait()
+        if pair + 2 == SEQS:
+            load("vw", value_weight, vw)
+            load("ow", out_weight.at[:, pl.ds(pl.multiple_of(c * HALF, HALF), HALF)], ow.at[c])
+            share_at = pl.multiple_of(c * HALF + z * SHARE, SHARE)
+            load("res_cols", residual.at[:, pl.ds(share_at, SHARE)], res_cols)
+            load("ids", ids, idv)
+            load("mg", mixer_gain, mg)
+            load("grt", group_router, grt)
+            load("ert", expert_router, ert)
+        for s in range(pair, pair + 2):
+            attend(s)
+    pl.semaphore_wait(barrier, 45)
+    swaps = [
+        remote(
+            out_weight.at[:, pl.ds(pl.multiple_of(other * HALF, HALF), HALF)],
+            ow.at[c],
+            w_ssem.at[0],
+            w_rsem.at[0],
+            ep,
+            partner,
+        ),
+        remote(gate_weight.at[other], gw.at[1], w_ssem.at[1], w_rsem.at[1], ep, partner),
+        remote(up_weight.at[other], uw.at[1], w_ssem.at[2], w_rsem.at[2], ep, partner),
+        remote(down_weight.at[other], dw.at[1], w_ssem.at[3], w_rsem.at[3], ep, partner),
+    ]
+    swaps[0].start()
 
     loads["vw"].wait()
     wide = dot(mixl[...], vw[...])
@@ -298,15 +317,17 @@
     def hv_copy(i):
         there = lax.rem(tp + i, N_TP)
         return remote(
-            hv_send.at[lax.div(there, 2)], hv_recv.at[tp], hv_ssem.at[i], hv_rsem.at[tp], ep, there
-        )
-
-    def hv_start(i, carry):
-        hv_copy(lax.rem(i + 7, N_TP - 1) + 1).start()
-        return carry
-
-    lax.fori_loop(0, N_TP - 1, hv_start, 0)
+            hv_send.at[lax.div(there, 2)], hv_recv.at[tp], hv_ssem, hv_rsem.at[tp], ep, there
+        )
+
+    for i in (8, 7, 9, 6, 10, 5, 11, 4, 12, 3, 13, 2, 14, 1, 15):
+        hv_copy(i).start()
     hv_recv[tp] = hv_send[z]
+    swaps[1].start()
+    swaps[2].start()
+    load("gw", gate_weight.at[c], gw.at[0])
+    load("uw", up_weight.at[c], uw.at[0])
+    load("dw", down_weight.at[c], dw.at[0])
 
     loads["ids"].wait()
     idr = idv[...]
@@ -336,7 +357,7 @@
     def hv_wait(i, carry):
         src = lax.rem(tp + i, N_TP)
         remote(
-            hv_send.at[0], hv_recv.at[src], hv_ssem.at[i], hv_rsem.at[src], ep, src
+            hv_send.at[0], hv_recv.at[src], hv_ssem, hv_rsem.at[src], ep, src
         ).wait_recv()
         return carry
 
@@ -353,32 +374,28 @@
         term = dot(dot(rows_k, heads_in).astype(BF16), ow[k])
         part = term if part is None else part + term
     for zz in range(NZ):
-        piece = part[:, zz * SHARE : (zz + 1) * SHARE]
-        acc[zz] = piece
-        rs_send[zz] = piece.astype(BF16)
-
-    order = (4, 3, 5, 2, 6, 1, 7)
-
-    def scatter(send, recv, ssem, rsem):
-        def copy(i):
-            to = ring(i)
-            return remote(
-                send.at[to], recv.at[z], ssem.at[i], rsem.at[z], ep, to * 2 + c
-            )
-
-        for i in order:
-            copy(i).start()
+        acc[zz] = part[:, zz * SHARE : (zz + 1) * SHARE]
+    for i in ORDER:
+        rs_send[i] = acc[ring(i)].astype(BF16)
+
+    def scatter_copy(send, recv, ssem, rsem, i):
+        return remote(send.at[i], recv.at[z], ssem.at[i], rsem.at[z], ep, ring(i) * 2 + c)
+
+    def scatter(send, recv, ssem, rsem, steps):
+        for i in steps:
+            scatter_copy(send, recv, ssem, rsem, i).start()
 
     def scatter_wait(send, recv, ssem, rsem, total):
-        for i in reversed(order):
+        for i in reversed(ORDER):
             src = ring(i)
             remote(
-                send.at[src], recv.at[src], ssem.at[i], rsem.at[src], ep, src * 2 + c
+                send.at[i], recv.at[src], ssem.at[i], rsem.at[src], ep, src * 2 + c
             ).wait_recv()
             total += recv[src].astype(F32)
         return total
 
-    scatter(rs_send, rs_recv, rs_ssem, rs_rsem)
+    scatter(rs_send, rs_recv, rs_ssem, rs_rsem, ORDER)
+    swaps[3].start()
     loads["res_cols"].wait()
     total = res_cols[...].astype(F32) + scatter_wait(rs_send, rs_recv, rs_ssem, rs_rsem, acc[z])
     after[z] = total.astype(BF16)
@@ -388,43 +405,44 @@
             after.at[src], after.at[src], ag_ssem.at[i], ag_rsem.at[src], ep, ring(i) * 2 + c
         )
 
-    for i in order:
+    for i in ORDER:
         ag_copy(i, z).start()
 
-    def place_slots(zz):
-        at = pl.ds(pl.multiple_of(zz * SHARE, SHARE), SHARE)
-        disp[:, at] = dot(sel[...], after[zz]).astype(BF16)
-
-    place_slots(z)
-    for i in reversed(order):
-        src = ring(i)
-        remote(
-            after.at[z], after.at[src], ag_ssem.at[i], ag_rsem.at[src], ep, src * 2 + c
-        ).wait_recv()
-        place_slots(src)
-
-    def x_copy(i, core):
+    mine = pl.ds(pl.multiple_of((ep * 2 + c) * CAP, CAP), CAP)
+    here = pl.ds(pl.multiple_of(ep * CAP, CAP), CAP)
+    theirs = pl.ds(pl.multiple_of((ep * 2 + other) * CAP, CAP), CAP)
+
+    def x_copy(n, i, core):
         there = lax.rem(ep + i, N_EP)
         at = pl.ds(pl.multiple_of((there * 2 + core) * CAP, CAP), CAP)
-        to = pl.ds(pl.multiple_of(ep * CAP, CAP), CAP)
+        cols = pl.ds(*spans(OUT_GROUPS)[n])
         return remote(
-            disp.at[at, :],
-            xin.at[c, to, :],
-            x_ssem.at[i * 2 + core],
-            x_rsem.at[ep * 2 + c],
+            disp.at[at, cols],
+            xin.at[c, here, cols],
+            x_ssem.at[n],
+            x_rsem.at[n, ep * 2 + c],
             there,
             z * 2 + core,
         )
 
-    def x_start(i, carry):
-        for core in range(2):
-            x_copy(i, core).start()
-        return carry
-
-    lax.fori_loop(1, N_EP, x_start, 0)
-    x_copy(0, other).start()
-    mine = pl.ds(pl.multiple_of((ep * 2 + c) * CAP, CAP), CAP)
-    here = pl.ds(pl.multiple_of(ep * CAP, CAP), CAP)
+    for n, group in enumerate(OUT_GROUPS):
+        base = spans(OUT_GROUPS)[n][0]
+        for place_at, i in enumerate(group):
+            src = ring(i)
+            if i:
+                remote(
+                    after.at[z], after.at[src], ag_ssem.at[i], ag_rsem.at[src], ep, src * 2 + c
+                ).wait_recv()
+            at = base + place_at * SHARE
+            disp[:, at : at + SHARE] = dot(sel[...], after[src]).astype(BF16)
+
+        def x_start(i, carry, n=n):
+            for core in range(2):
+                x_copy(n, i, core).start()
+            return carry
+
+        lax.fori_loop(1, N_EP, x_start, 0)
+        x_copy(n, 0, other).start()
     xin[c, here, :] = disp[mine, :]
     to_partner = remote(after, after_other, ot_ssem, ot_rsem, ep, partner)
     to_partner.start()
@@ -438,7 +456,8 @@
         full[:, at] = after[zz]
         at = pl.ds(pl.multiple_of(other * HALF + zz * SHARE, SHARE), SHARE)
         full[:, at] = after_other[zz]
-    gain = mg[...].astype(F32)
+    gain = mg[...].astype(F32)[None, :]
+    gain2[...] = gain
     rows = full[...].astype(F32)
     inv = lax.rsqrt(jnp.mean(rows * rows, axis=1, keepdims=True) + EPS)
     expert_in = (rows * inv * gain).astype(BF16)
@@ -460,35 +479,37 @@
     comb[0:ROWS, :] = high
     comb[ROWS:, :] = (weights - high.astype(F32)).astype(BF16)
 
-    def x_wait(i, carry):
+    def x_arrival(n, i, core):
         src = lax.rem(ep + i, N_EP)
         at = pl.ds(pl.multiple_of(src * CAP, CAP), CAP)
-        for core in range(2):
-            remote(
-                disp.at[at, :],
-                xin.at[core, at, :],
-                x_ssem.at[i * 2 + core],
-                x_rsem.at[src * 2 + core],
-                src,
-                z * 2 + core,
-            ).wait_recv()
-        return carry
-
-    remote(
-        disp.at[here, :],
-        xin.at[other, here, :],
-        x_ssem.at[other],
-        x_rsem.at[ep * 2 + other],
-        ep,
-        partner,
-    ).wait_recv()
-    lax.fori_loop(1, N_EP, x_wait, 0)
+        cols = pl.ds(*spans(OUT_GROUPS)[n])
+        return remote(
+            disp.at[at, cols],
+            xin.at[core, at, cols],
+            x_ssem.at[n],
+            x_rsem.at[n, src * 2 + core],
+            src,
+            z * 2 + core,
+        )
+
+    for n in range(len(OUT_GROUPS)):
+
+        def x_wait(i, carry, n=n):
+            for core in range(2):
+                x_arrival(n, i, core).wait_recv()
+            return carry
+
+        x_arrival(n, 0, other).wait_recv()
+        lax.fori_loop(1, N_EP, x_wait, 0)
     x0 = xin[0].astype(F32)
     x1 = xin[1].astype(F32)
     square = jnp.sum(x0 * x0, axis=1, keepdims=True) + jnp.sum(x1 * x1, axis=1, keepdims=True)
     inv = lax.rsqrt(square * (1.0 / D) + EPS)
-    xn[:, 0:HALF] = (x0 * inv * gain[:, 0:HALF]).astype(BF16)
-    xn[:, HALF:] = (x1 * inv * gain[:, HALF:]).astype(BF16)
+    for core in range(2):
+        for place_at, i in enumerate(sum(OUT_GROUPS, ())):
+            at = pl.ds(pl.multiple_of(core * HALF + ring(i) * SHARE, SHARE), SHARE)
+            piece = xin[core, :, place_at * SHARE : (place_at + 1) * SHARE].astype(F32)
+            xn[:, at] = (piece * inv * gain2[:, at]).astype(BF16)
     acts = []
     for name in ("gw", "uw", "dw"):
         loads[name].wait()
@@ -499,63 +520,71 @@
         u = dot(xn[...], uw[k])
         acts.append((g * (1.0 / (1.0 + jnp.exp(-g))) * u).astype(BF16))
 
-    def y_copy(i, half):
+    def y_copy(n, i, half):
         there = lax.rem(ep + i, N_EP)
         at = pl.ds(pl.multiple_of(there * CAP, CAP), CAP)
+        cols = pl.ds(*spans(BACK_GROUPS)[n])
         return remote(
-            ret.at[half, at, :],
-            yin.at[mine, :],
-            y_ssem.at[i * 2 + half],
-            y_rsem.at[ep * 2 + c],
+            ret.at[half, at, cols],
+            yin.at[mine, cols],
+            y_ssem.at[n],
+            y_rsem.at[n, ep * 2 + c],
             there,
             z * 2 + half,
         )
 
-    for half in range(2):
-        cols = slice(half * HALF, (half + 1) * HALF)
-        ret[half] = (dot(acts[0], dw[0, :, cols]) + dot(acts[1], dw[1, :, cols])).astype(BF16)
-
-        def y_start(i, carry, half=half):
-            y_copy(i, half).start()
+    for n, group in enumerate(BACK_GROUPS):
+        base = spans(BACK_GROUPS)[n][0]
+        for half in range(2):
+            for place_at, i in enumerate(group):
+                at = pl.ds(pl.multiple_of(half * HALF + ring(i) * SHARE, SHARE), SHARE)
+                to = base + place_at * SHARE
+                ret[half, :, to : to + SHARE] = (
+                    dot(acts[0], dw[0, :, at]) + dot(acts[1], dw[1, :, at])
+                ).astype(BF16)
+
+        def y_start(i, carry, n=n):
+            for half in range(2):
+                y_copy(n, i, half).start()
             return carry
 
         lax.fori_loop(1, N_EP, y_start, 0)
-    y_copy(0, other).start()
+        y_copy(n, 0, other).start()
     yin[mine, :] = ret[c, here, :]
 
-    def y_wait(i, carry):
+    def y_arrival(n, i, core):
         src = lax.rem(ep + i, N_EP)
-        for core in range(2):
-            at = pl.ds(pl.multiple_of((src * 2 + core) * CAP, CAP), CAP)
-            remote(
-                ret.at[core, here, :],
-                yin.at[at, :],
-                y_ssem.at[i * 2 + core],
-                y_rsem.at[src * 2 + core],
-                src,
-                z * 2 + core,
-            ).wait_recv()
-        return carry
-
-    theirs = pl.ds(pl.multiple_of((ep * 2 + other) * CAP, CAP), CAP)
-    remote(
-        ret.at[other, here, :],
-        yin.at[theirs, :],
-        y_ssem.at[other],
-        y_rsem.at[ep * 2 + other],
-        ep,
-        partner,
-    ).wait_recv()
-    lax.fori_loop(1, N_EP, y_wait, 0)
-
-    both = dot(comb[...], yin[...])
-    moe = both[0:ROWS] + both[ROWS:]
-    for zz in range(NZ):
-        piece = moe[:, zz * SHARE : (zz + 1) * SHARE]
-        acc[zz] = piece
-        rs2_send[zz] = piece.astype(BF16)
-    scatter(rs2_send, rs2_recv, rs2_ssem, rs2_rsem)
-    total = after[z].astype(F32) + scatter_wait(rs2_send, rs2_recv, rs2_ssem, rs2_rsem, acc[z])
+        at = pl.ds(pl.multiple_of((src * 2 + core) * CAP, CAP), CAP)
+        cols = pl.ds(*spans(BACK_GROUPS)[n])
+        return remote(
+            ret.at[core, here, cols],
+            yin.at[at, cols],
+            y_ssem.at[n],
+            y_rsem.at[n, src * 2 + core],
+            src,
+            z * 2 + core,
+        )
+
+    for n, group in enumerate(BACK_GROUPS):
+
+        def y_wait(i, carry, n=n):
+            for core in range(2):
+                y_arrival(n, i, core).wait_recv()
+            return carry
+
+        y_arrival(n, 0, other).wait_recv()
+        lax.fori_loop(1, N_EP, y_wait, 0)
+        base, width = spans(BACK_GROUPS)[n]
+        both = dot(comb[...], yin[:, base : base + width])
+        moe = both[0:ROWS] + both[ROWS:]
+        for place_at, i in enumerate(group):
+            piece = moe[:, place_at * SHARE : (place_at + 1) * SHARE]
+            if i:
+                rs2_send[i] = piece.astype(BF16)
+                scatter(rs2_send, rs2_recv, rs2_ssem, rs2_rsem, (i,))
+            else:
+                acc[0] = piece
+    total = after[z].astype(F32) + scatter_wait(rs2_send, rs2_recv, rs2_ssem, rs2_rsem, acc[0])
     fin[c, z] = total.astype(BF16)
 
     def f_copy(i):
@@ -566,10 +595,10 @@
     def p_copy(zz, i):
         return remote(fin.at[c, zz], fin.at[c, zz], p_ssem.at[i], p_rsem.at[zz], ep, partner)
 
-    for i in order:
+    for i in ORDER:
         f_copy(i).start()
     p_copy(z, 0).start()
-    for i in reversed(order):
+    for i in reversed(ORDER):
         src = ring(i)
         remote(
             fin.at[c, src], fin.at[c, src], f_ssem.at[i], f_rsem.at[src], ep, src * 2 + c
@@ -582,7 +611,7 @@
 
     for zz in range(NZ):
         spread(c, zz)
-    for i in (0,) + order[::-1]:
+    for i in (0,) + ORDER[::-1]:
         src = ring(i)
         remote(
             fin.at[other, src], fin.at[other, src], p_ssem.at[i], p_rsem.at[src], ep, partner
@@ -591,33 +620,35 @@
 
     for copy in swaps:
         copy.wait_send()
-
-    def hv_drain(i, carry):
-        hv_copy(i).wait_send()
-        return carry
-
-    lax.fori_loop(1, N_TP, hv_drain, 0)
-    for i in order:
-        to = ring(i)
-        remote(rs_send.at[to], rs_recv.at[z], rs_ssem.at[i], rs_rsem.at[z], ep, to * 2 + c).wait_send()
+    remote(
+        hv_recv.at[0 : N_TP - 1], hv_recv.at[0 : N_TP - 1], hv_ssem, hv_rsem.at[0], ep, partner
+    ).wait_send()
+    for i in ORDER:
+        scatter_copy(rs_send, rs_recv, rs_ssem, rs_rsem, i).wait_send()
         ag_copy(i, z).wait_send()
-        remote(
-            rs2_send.at[to], rs2_recv.at[z], rs2_ssem.at[i], rs2_rsem.at[z], ep, to * 2 + c
-        ).wait_send()
+        scatter_copy(rs2_send, rs2_recv, rs2_ssem, rs2_rsem, i).wait_send()
         f_copy(i).wait_send()
         p_copy(ring(i), i).wait_send()
     p_copy(z, 0).wait_send()
     to_partner.wait_send()
-    x_copy(0, other).wait_send()
-    y_copy(0, other).wait_send()
-
-    def xy_drain(i, carry):
-        for core in range(2):
-            x_copy(i, core).wait_send()
-            y_copy(i, core).wait_send()
-        return carry
-
-    lax.fori_loop(1, N_EP, xy_drain, 0)
+    sent = pl.ds(0, OTHERS * CAP)
+    for n, span in enumerate(spans(OUT_GROUPS)):
+        part_of = disp.at[sent, pl.ds(*span)]
+        remote(part_of, part_of, x_ssem.at[n], x_rsem.at[n, 0], ep, partner).wait_send()
+    for n, span in enumerate(spans(BACK_GROUPS)):
+        part_of = yin.at[sent, pl.ds(*span)]
+        remote(part_of, part_of, y_ssem.at[n], y_rsem.at[n, 0], ep, partner).wait_send()
+
+
+def write_out(a, b, c, a_out, b_out, c_out, sem):
+    copies = [
+        pltpu.make_async_copy(src, dst, sem.at[i])
+        for i, (src, dst) in enumerate(((a, a_out), (b, b_out), (c, c_out)))
+    ]
+    for copy in copies:
+        copy.start()
+    for copy in copies:
+        copy.wait()
 
 
 def on_device(
@@ -643,33 +674,32 @@
 ):
     anywhere = pl.BlockSpec(memory_space=pl.ANY)
     vmem = pl.BlockSpec(memory_space=pltpu.VMEM)
-    smem = pl.BlockSpec(memory_space=pltpu.SMEM)
     dma = pltpu.SemaphoreType.DMA
     in_specs = [anywhere] * 19
-    in_specs[3] = smem
-    return pl.pallas_call(
+    results = pl.pallas_call(
         kernel,
         out_shape=(
-            jax.ShapeDtypeStruct((ROWS, D), BF16),
-            jax.ShapeDtypeStruct((SEQS, KV), BF16),
-            jax.ShapeDtypeStruct((SEQS, ROPE), BF16),
+            pltpu.VMEM((ROWS, D), BF16),
+            pltpu.VMEM((SEQS, KV), BF16),
+            pltpu.VMEM((SEQS, ROPE), BF16),
         ),
         in_specs=in_specs,
         out_specs=(vmem, vmem, vmem),
         scratch_shapes=[
+            pltpu.SMEM((SEQS,), I32),
             pltpu.VMEM((8, D), BF16),
             pltpu.VMEM((ROWS, SHARE), BF16),
             pltpu.VMEM((SEQS, LEN, KV), BF16),
             pltpu.VMEM((SEQS, ROPE, LEN), BF16),
             pltpu.VMEM((SEQS, H, KV), BF16),
             pltpu.VMEM((SEQS, H, ROPE), BF16),
-            pltpu.VMEM((1, D), BF16),
+            pltpu.VMEM((D,), BF16),
             pltpu.VMEM((D, KV), BF16),
-            pltpu.VMEM((1, KV), BF16),
+            pltpu.VMEM((KV,), BF16),
             pltpu.VMEM((ROPE, D), BF16),
             pltpu.VMEM((KV, D), BF16),
             pltpu.VMEM((2, SHARE, HALF), BF16),
-            pltpu.VMEM((1, D), BF16),
+            pltpu.VMEM((D,), BF16),
             pltpu.VMEM((GROUPS, D), BF16),
             pltpu.VMEM((EXPERTS, D), BF16),
             pltpu.VMEM((2, ROWS), I32),
@@ -695,10 +725,12 @@
             pltpu.VMEM((NZ, ROWS, SHARE), BF16),
             pltpu.VMEM((NZ, ROWS, SHARE), BF16),
             pltpu.VMEM((2, NZ, ROWS, SHARE), BF16),
+            pltpu.VMEM((1, D), F32),
+            pltpu.VMEM((SEQS, KV, LEN), BF16),
             dma((32,)),
             dma((4,)),
             dma((4,)),
-            dma((N_TP,)),
+            dma,
             dma((N_TP,)),
             dma((NZ,)),
             dma((NZ,)),
@@ -706,10 +738,10 @@
             dma((NZ,)),
             dma,
             dma,
-            dma((2 * N_EP,)),
-            dma((2 * N_EP,)),
-            dma((2 * N_EP,)),
-            dma((2 * N_EP,)),
+            dma((len(OUT_GROUPS),)),
+            dma((len(OUT_GROUPS), 2 * N_EP)),
+            dma((len(BACK_GROUPS),)),
+            dma((len(BACK_GROUPS), 2 * N_EP)),
             dma((NZ,)),
             dma((NZ,)),
             dma((NZ,)),
@@ -727,13 +759,13 @@
         lengths,
         query_latent,
         query_rope,
-        norm_gain.reshape(1, D),
+        norm_gain,
         latent_weight,
-        latent_gain.reshape(1, KV),
+        latent_gain,
         rope_weight,
         value_weight,
         out_weight,
-        mixer_gain.reshape(1, D),
+        mixer_gain,
         group_router.T,
         expert_router.T,
         expert_ids.T,
@@ -741,6 +773,18 @@
         up_weight,
         down_weight,
     )
+    return pl.pallas_call(
+        write_out,
+        out_shape=(
+            jax.ShapeDtypeStruct((ROWS, D), BF16),
+            jax.ShapeDtypeStruct((SEQS, KV), BF16),
+            jax.ShapeDtypeStruct((SEQS, ROPE), BF16),
+        ),
+        in_specs=[vmem] * 3,
+        out_specs=(anywhere,) * 3,
+        scratch_shapes=[dma((3,))],
+        compiler_params=pltpu.CompilerParams(vmem_limit_bytes=1024 * 1024),
+    )(*results)
 
 
 def solution(mesh):

time: 71.3 us -> 60.8 us (0.85)
  local copies, waits for them, and re-layouts: 7.97 us -> 0 us
  Pallas kernels: 62.3 us -> 60.1 us
    unnamed x3 -> x0, local copies, waits for them, and re-layouts: 4.17 us -> none
    reshape x3 -> x0, local copies, waits for them, and re-layouts: 3.8 us -> none  [the longest x1 1.29 us: on_device(): norm_gain.reshape(1, D)]
    pallas_call x1 -> x2, Pallas kernels: 62.3 us -> 60.1 us  [the longest x1 59.3 us: on_device(): pl.pallas_call(kernel, out_shape=(pltpu.VMEM((ROWS, D), BF16), pltpu.VMEM...]
where the time goes in v2:
time: 60.8 us; the launch traced here: 60.7 us
  Pallas kernels  60.1 us (99%)
  between operations  0.65 us (1%)
    pallas_call x1, Pallas kernels, on_device(): pl.pallas_call(kernel, out_shape=(pltpu.VMEM((ROWS, D), BF16), pltpu.VMEM...  59.3 us

profile of v2, /device:TPU:1, one launch (start us, length us, event | category | flops | bytes accessed | tf_op | source)
XLA Modules:
  0.0 60.7 jit_solution(6084175973440767967)
XLA Ops:
  0.6 59.3 %shard_map.202 = (bf16[64,2048]{1,0:T(8,128)(2,1)S(1)}, bf16[4,256]{1,0:T(4,128)(2,1)S(1)}, bf16[4,32]{1,0:T(4,128)(2,1)S(1)}) custom-call(bf16[64,2048]{1,0:T(8,128)(2,1)} %residual.1, bf16[4,2048,256]{2,1,0:T(8,128)(2,1)} %cache_latent.1, bf16[4,32,2048]{2,1,0:T(8,128)(2,1)} %cache_rope.1, s32[4]{0:T(128)} %lengths_in.1, bf16[4,32,256]{2,1,0:T(8,128)(2,1)} %query_latent.1, ...), custom_call_target="tpu_custom_call" | custom-call | tf_op jit(solution)/shard_map/pallas_call | solution.py:679
  60.0 0.7 %shard_map.203 = (bf16[64,2048]{1,0:T(8,128)(2,1)}, bf16[4,256]{1,0:T(4,128)(2,1)}, bf16[4,32]{1,0:T(4,128)(2,1)}) custom-call(bf16[64,2048]{1,0:T(8,128)(2,1)S(1)} %get-tuple-element.6.a, bf16[4,256]{1,0:T(4,128)(2,1)S(1)} %get-tuple-element.7.b, bf16[4,32]{1,0:T(4,128)(2,1)S(1)} %get-tuple-element.8.c), custom_call_target="tpu_custom_call" | custom-call | tf_op jit(solution)/shard_map/pallas_call | solution.py:776

commit v3 on v2

--- a/solution.py
+++ b/solution.py
@@ -36,8 +36,15 @@
 EPS = 1e-06
 ROPE_BASE = 10000.0
 ORDER = (4, 3, 5, 2, 6, 1, 7)
-OUT_GROUPS = ((0, 1, 7), (2, 6), (3, 5, 4))
-BACK_GROUPS = ((4, 3, 5, 2), (6, 1, 7, 0))
+OUT_GROUPS = ((0,), (1, 7), (2, 6), (3, 5, 4))
+BACK_GROUPS = ((4, 3, 5), (2, 6), (1, 7, 0))
+
+FAR_FIRST = tuple(
+    sorted(
+        ((a, b) for a in range(4) for b in range(4) if a or b),
+        key=lambda step: -sum(min(v, 4 - v) for v in step),
+    )
+)
 
 
 def spans(groups):
@@ -115,7 +122,6 @@
     sel,
     disp,
     xin,
-    xn,
     ret,
     yin,
     comb,
@@ -124,6 +130,7 @@
     fin,
     gain2,
     lt,
+    early,
     local_sem,
     w_ssem,
     w_rsem,
@@ -189,6 +196,8 @@
         copy.start()
         loads[name] = copy
 
+    load("ql", query_latent, ql)
+    load("cl0", cache_latent.at[0:2], cl.at[0:2])
     load("len", lengths_in, lengths)
     load("res8", residual.at[pl.ds(pl.multiple_of(z * 8, 8), 8), :], res8)
     load("ng", norm_gain, ng)
@@ -196,25 +205,26 @@
     load("rw", rope_weight, rw)
     load("qr", query_rope, qr)
     load("lw", latent_weight, lw)
-    load("ql", query_latent, ql)
-    for s in range(SEQS):
-        load(f"cr{s}", cache_rope.at[s], cr.at[s])
-        load(f"cl{s}", cache_latent.at[s], cl.at[s])
+    load("cr", cache_rope, cr)
+    load("cl2", cache_latent.at[2:4], cl.at[2:4])
 
     lax.fori_loop(1, N_TP, signal_tp, 0)
     lax.fori_loop(1, N_EP, signal_ep, 0)
 
-    loads["res8"].wait()
-    loads["ng"].wait()
+    loads["ql"].wait()
+    loads["cl0"].wait()
+    for s in range(2):
+        lt[s] = cl[s].T
+        early[s] = dot(ql[s], lt[s])
+
+    for name in ("len", "res8", "ng", "lg", "rw", "qr", "lw", "cr", "cl2"):
+        loads[name].wait()
     rows = res8[...].astype(F32)
     inv = lax.rsqrt(jnp.mean(rows * rows, axis=1, keepdims=True) + EPS)
     normed = (rows * inv * ng[...].astype(F32)[None, :]).astype(BF16)
-    loads["rw"].wait()
     rope_raw = dot_t(normed, rw[...])
-    loads["lw"].wait()
     latent_raw = dot(normed, lw[...])
     inv = lax.rsqrt(jnp.mean(latent_raw * latent_raw, axis=1, keepdims=True) + EPS)
-    loads["lg"].wait()
     latent8 = latent_raw * inv * lg[...].astype(F32)[None, :]
 
     def own_rows(v):
@@ -225,7 +235,6 @@
     new_latent_out[...] = new_latent[0:SEQS]
     rope_own = own_rows(rope_raw)
 
-    loads["len"].wait()
     lane = iota((8, ROPE), 1)
     row = iota((8, ROPE), 0)
     place = lax.rem(lane, ROPE // 2).astype(F32)
@@ -247,15 +256,17 @@
     new_rope_f = new_rope.astype(F32)
 
     scale = (NOPE + ROPE) ** (-0.5)
-    loads["qr"].wait()
-    loads["ql"].wait()
     def attend(s):
         u = qr[s].astype(F32)
         turned = (u * cos[s : s + 1] + swapped(u) * sin[s : s + 1]).astype(BF16)
         q = ql[s]
         latents = cl[s]
-        lt[s] = latents.T
-        score = (dot(q, lt[s]) + dot(turned, cr[s])) * scale
+        if s < 2:
+            score = early[s]
+        else:
+            lt[s] = latents.T
+            score = dot(q, lt[s])
+        score = (score + dot(turned, cr[s])) * scale
         keep = iota((H, LEN), 1) < lengths[s]
         score = jnp.where(keep, score, -jnp.inf)
         fresh = (
@@ -271,21 +282,16 @@
         mixed = dot(weight, latents) + fresh_w * new_latent_f[s : s + 1]
         mixl[s * H : (s + 1) * H, :] = mixed.astype(BF16)
 
-    for pair in range(0, SEQS, 2):
-        for s in range(pair, pair + 2):
-            loads[f"cr{s}"].wait()
-            loads[f"cl{s}"].wait()
-        if pair + 2 == SEQS:
-            load("vw", value_weight, vw)
-            load("ow", out_weight.at[:, pl.ds(pl.multiple_of(c * HALF, HALF), HALF)], ow.at[c])
-            share_at = pl.multiple_of(c * HALF + z * SHARE, SHARE)
-            load("res_cols", residual.at[:, pl.ds(share_at, SHARE)], res_cols)
-            load("ids", ids, idv)
-            load("mg", mixer_gain, mg)
-            load("grt", group_router, grt)
-            load("ert", expert_router, ert)
-        for s in range(pair, pair + 2):
-            attend(s)
+    load("vw", value_weight, vw)
+    load("ow", out_weight.at[:, pl.ds(pl.multiple_of(c * HALF, HALF), HALF)], ow.at[c])
+    share_at = pl.multiple_of(c * HALF + z * SHARE, SHARE)
+    load("res_cols", residual.at[:, pl.ds(share_at, SHARE)], res_cols)
+    load("ids", ids, idv)
+    load("mg", mixer_gain, mg)
+    load("grt", group_router, grt)
+    load("ert", expert_router, ert)
+    for s in range(SEQS):
+        attend(s)
     pl.semaphore_wait(barrier, 45)
     swaps = [
         remote(
@@ -317,7 +323,7 @@
     def hv_copy(i):
         there = lax.rem(tp + i, N_TP)
         return remote(
-            hv_send.at[lax.div(there, 2)], hv_recv.at[tp], hv_ssem, hv_rsem.at[tp], ep, there
+            hv_send.at[lax.div(there, 2)], hv_recv.at[tp], hv_ssem, hv_rsem, ep, there
         )
 
     for i in (8, 7, 9, 6, 10, 5, 11, 4, 12, 3, 13, 2, 14, 1, 15):
@@ -354,14 +360,8 @@
         chosen += (jnp.broadcast_to(to_row(slot_col[k]), (SLOTS, ROWS)) == slot_iota).astype(F32)
     sel[...] = chosen.astype(BF16)
 
-    def hv_wait(i, carry):
-        src = lax.rem(tp + i, N_TP)
-        remote(
-            hv_send.at[0], hv_recv.at[src], hv_ssem, hv_rsem.at[src], ep, src
-        ).wait_recv()
-        return carry
-
-    lax.fori_loop(1, N_TP, hv_wait, 0)
+    all_heads = hv_recv.at[0 : N_TP - 1]
+    remote(all_heads, all_heads, hv_ssem, hv_rsem, ep, partner).wait_recv()
 
     loads["ow"].wait()
     swaps[0].wait_recv()
@@ -379,70 +379,72 @@
         rs_send[i] = acc[ring(i)].astype(BF16)
 
     def scatter_copy(send, recv, ssem, rsem, i):
-        return remote(send.at[i], recv.at[z], ssem.at[i], rsem.at[z], ep, ring(i) * 2 + c)
+        return remote(send.at[i], recv.at[z], ssem, rsem, ep, ring(i) * 2 + c)
 
     def scatter(send, recv, ssem, rsem, steps):
         for i in steps:
             scatter_copy(send, recv, ssem, rsem, i).start()
 
-    def scatter_wait(send, recv, ssem, rsem, total):
-        for i in reversed(ORDER):
-            src = ring(i)
-            remote(
-                send.at[i], recv.at[src], ssem.at[i], rsem.at[src], ep, src * 2 + c
-            ).wait_recv()
-            total += recv[src].astype(F32)
+    def scatter_all(recv, ssem, rsem):
+        seven = recv.at[0 : NZ - 1]
+        return remote(seven, seven, ssem, rsem, ep, partner)
+
+    def scatter_wait(recv, ssem, rsem, total):
+        scatter_all(recv, ssem, rsem).wait_recv()
+        for i in ORDER:
+            total += recv[ring(i)].astype(F32)
         return total
 
     scatter(rs_send, rs_recv, rs_ssem, rs_rsem, ORDER)
     swaps[3].start()
     loads["res_cols"].wait()
-    total = res_cols[...].astype(F32) + scatter_wait(rs_send, rs_recv, rs_ssem, rs_rsem, acc[z])
+    total = res_cols[...].astype(F32) + scatter_wait(rs_recv, rs_ssem, rs_rsem, acc[z])
     after[z] = total.astype(BF16)
 
-    def ag_copy(i, src):
+    def group_of(i):
+        return [i in group for group in OUT_GROUPS].index(True)
+
+    def ag_copy(i):
         return remote(
-            after.at[src], after.at[src], ag_ssem.at[i], ag_rsem.at[src], ep, ring(i) * 2 + c
+            after.at[z], after.at[z], ag_ssem, ag_rsem.at[group_of(NZ - i)], ep, ring(i) * 2 + c
         )
 
     for i in ORDER:
-        ag_copy(i, z).start()
+        ag_copy(i).start()
 
     mine = pl.ds(pl.multiple_of((ep * 2 + c) * CAP, CAP), CAP)
     here = pl.ds(pl.multiple_of(ep * CAP, CAP), CAP)
     theirs = pl.ds(pl.multiple_of((ep * 2 + other) * CAP, CAP), CAP)
 
-    def x_copy(n, i, core):
-        there = lax.rem(ep + i, N_EP)
+    def away(step):
+        down, right = step
+        return lax.rem(lax.div(ep, 4) + down, 4) * 4 + lax.rem(ep + right, 4)
+
+    def x_copy(n, step, core):
+        there = away(step)
         at = pl.ds(pl.multiple_of((there * 2 + core) * CAP, CAP), CAP)
         cols = pl.ds(*spans(OUT_GROUPS)[n])
         return remote(
             disp.at[at, cols],
             xin.at[c, here, cols],
             x_ssem.at[n],
-            x_rsem.at[n, ep * 2 + c],
+            x_rsem.at[n],
             there,
             z * 2 + core,
         )
 
     for n, group in enumerate(OUT_GROUPS):
         base = spans(OUT_GROUPS)[n][0]
+        come = after.at[0 : max(1, len(group) - (0 in group))]
+        if group != (0,):
+            remote(come, come, ag_ssem, ag_rsem.at[n], ep, partner).wait_recv()
         for place_at, i in enumerate(group):
-            src = ring(i)
-            if i:
-                remote(
-                    after.at[z], after.at[src], ag_ssem.at[i], ag_rsem.at[src], ep, src * 2 + c
-                ).wait_recv()
             at = base + place_at * SHARE
-            disp[:, at : at + SHARE] = dot(sel[...], after[src]).astype(BF16)
-
-        def x_start(i, carry, n=n):
+            disp[:, at : at + SHARE] = dot(sel[...], after[ring(i)]).astype(BF16)
+        for step in FAR_FIRST:
             for core in range(2):
-                x_copy(n, i, core).start()
-            return carry
-
-        lax.fori_loop(1, N_EP, x_start, 0)
-        x_copy(n, 0, other).start()
+                x_copy(n, step, core).start()
+        x_copy(n, (0, 0), other).start()
     xin[c, here, :] = disp[mine, :]
     to_partner = remote(after, after_other, ot_ssem, ot_rsem, ep, partner)
     to_partner.start()
@@ -479,56 +481,53 @@
     comb[0:ROWS, :] = high
     comb[ROWS:, :] = (weights - high.astype(F32)).astype(BF16)
 
-    def x_arrival(n, i, core):
-        src = lax.rem(ep + i, N_EP)
-        at = pl.ds(pl.multiple_of(src * CAP, CAP), CAP)
-        cols = pl.ds(*spans(OUT_GROUPS)[n])
-        return remote(
-            disp.at[at, cols],
-            xin.at[core, at, cols],
-            x_ssem.at[n],
-            x_rsem.at[n, src * 2 + core],
-            src,
-            z * 2 + core,
-        )
-
-    for n in range(len(OUT_GROUPS)):
-
-        def x_wait(i, carry, n=n):
-            for core in range(2):
-                x_arrival(n, i, core).wait_recv()
-            return carry
-
-        x_arrival(n, 0, other).wait_recv()
-        lax.fori_loop(1, N_EP, x_wait, 0)
-    x0 = xin[0].astype(F32)
-    x1 = xin[1].astype(F32)
-    square = jnp.sum(x0 * x0, axis=1, keepdims=True) + jnp.sum(x1 * x1, axis=1, keepdims=True)
-    inv = lax.rsqrt(square * (1.0 / D) + EPS)
-    for core in range(2):
-        for place_at, i in enumerate(sum(OUT_GROUPS, ())):
-            at = pl.ds(pl.multiple_of(core * HALF + ring(i) * SHARE, SHARE), SHARE)
-            piece = xin[core, :, place_at * SHARE : (place_at + 1) * SHARE].astype(F32)
-            xn[:, at] = (piece * inv * gain2[:, at]).astype(BF16)
+    sent = pl.ds(0, OTHERS * CAP)
+
+    def x_all(n):
+        part_of = disp.at[sent, pl.ds(*spans(OUT_GROUPS)[n])]
+        return remote(part_of, part_of, x_ssem.at[n], x_rsem.at[n], ep, partner)
+
+    def y_all(n):
+        part_of = yin.at[sent, pl.ds(*spans(BACK_GROUPS)[n])]
+        return remote(part_of, part_of, y_ssem.at[n], y_rsem.at[n], ep, partner)
+
+    for name in ("gw", "uw"):
+        loads[name].wait()
+    swaps[1].wait_recv()
+    swaps[2].wait_recv()
+    products = [0.0, 0.0, 0.0, 0.0]
+    square = 0.0
+    for n, group in enumerate(OUT_GROUPS):
+        x_all(n).wait_recv()
+        base = spans(OUT_GROUPS)[n][0]
+        for core in range(2):
+            for place_at, i in enumerate(group):
+                at = pl.ds(pl.multiple_of(core * HALF + ring(i) * SHARE, SHARE), SHARE)
+                to = base + place_at * SHARE
+                piece = xin[core, :, to : to + SHARE].astype(F32)
+                square += piece * piece
+                scaled = (piece * gain2[:, at]).astype(BF16)
+                for k in range(2):
+                    products[k] += dot(scaled, gw[k, at, :])
+                    products[2 + k] += dot(scaled, uw[k, at, :])
+    inv = lax.rsqrt(jnp.sum(square, axis=1, keepdims=True) * (1.0 / D) + EPS)
     acts = []
-    for name in ("gw", "uw", "dw"):
-        loads[name].wait()
-    for copy in swaps[1:]:
-        copy.wait_recv()
     for k in range(2):
-        g = dot(xn[...], gw[k])
-        u = dot(xn[...], uw[k])
+        g = products[k] * inv
+        u = products[2 + k] * inv
         acts.append((g * (1.0 / (1.0 + jnp.exp(-g))) * u).astype(BF16))
-
-    def y_copy(n, i, half):
-        there = lax.rem(ep + i, N_EP)
+    loads["dw"].wait()
+    swaps[3].wait_recv()
+
+    def y_copy(n, step, half):
+        there = away(step)
         at = pl.ds(pl.multiple_of(there * CAP, CAP), CAP)
         cols = pl.ds(*spans(BACK_GROUPS)[n])
         return remote(
             ret.at[half, at, cols],
             yin.at[mine, cols],
             y_ssem.at[n],
-            y_rsem.at[n, ep * 2 + c],
+            y_rsem.at[n],
             there,
             z * 2 + half,
         )
@@ -543,37 +542,14 @@
                     dot(acts[0], dw[0, :, at]) + dot(acts[1], dw[1, :, at])
                 ).astype(BF16)
 
-        def y_start(i, carry, n=n):
+        for step in FAR_FIRST:
             for half in range(2):
-                y_copy(n, i, half).start()
-            return carry
-
-        lax.fori_loop(1, N_EP, y_start, 0)
-        y_copy(n, 0, other).start()
+                y_copy(n, step, half).start()
+        y_copy(n, (0, 0), other).start()
     yin[mine, :] = ret[c, here, :]
 
-    def y_arrival(n, i, core):
-        src = lax.rem(ep + i, N_EP)
-        at = pl.ds(pl.multiple_of((src * 2 + core) * CAP, CAP), CAP)
-        cols = pl.ds(*spans(BACK_GROUPS)[n])
-        return remote(
-            ret.at[core, here, cols],
-            yin.at[at, cols],
-            y_ssem.at[n],
-            y_rsem.at[n, src * 2 + core],
-            src,
-            z * 2 + core,
-        )
-
     for n, group in enumerate(BACK_GROUPS):
-
-        def y_wait(i, carry, n=n):
-            for core in range(2):
-                y_arrival(n, i, core).wait_recv()
-            return carry
-
-        y_arrival(n, 0, other).wait_recv()
-        lax.fori_loop(1, N_EP, y_wait, 0)
+        y_all(n).wait_recv()
         base, width = spans(BACK_GROUPS)[n]
         both = dot(comb[...], yin[:, base : base + width])
         moe = both[0:ROWS] + both[ROWS:]
@@ -584,26 +560,26 @@
                 scatter(rs2_send, rs2_recv, rs2_ssem, rs2_rsem, (i,))
             else:
                 acc[0] = piece
-    total = after[z].astype(F32) + scatter_wait(rs2_send, rs2_recv, rs2_ssem, rs2_rsem, acc[0])
+    total = after[z].astype(F32) + scatter_wait(rs2_recv, rs2_ssem, rs2_rsem, acc[0])
     fin[c, z] = total.astype(BF16)
 
     def f_copy(i):
         return remote(
-            fin.at[c, z], fin.at[c, z], f_ssem.at[i], f_rsem.at[z], ep, ring(i) * 2 + c
+            fin.at[c, z], fin.at[c, z], f_ssem, f_rsem.at[z], ep, ring(i) * 2 + c
         )
 
-    def p_copy(zz, i):
-        return remote(fin.at[c, zz], fin.at[c, zz], p_ssem.at[i], p_rsem.at[zz], ep, partner)
+    def p_copy(zz):
+        return remote(fin.at[c, zz], fin.at[c, zz], p_ssem, p_rsem, ep, partner)
 
     for i in ORDER:
         f_copy(i).start()
-    p_copy(z, 0).start()
+    p_copy(z).start()
     for i in reversed(ORDER):
         src = ring(i)
         remote(
-            fin.at[c, src], fin.at[c, src], f_ssem.at[i], f_rsem.at[src], ep, src * 2 + c
+            fin.at[c, src], fin.at[c, src], f_ssem, f_rsem.at[src], ep, src * 2 + c
         ).wait_recv()
-        p_copy(src, i).start()
+        p_copy(src).start()
 
     def spread(core, zz):
         at = pl.ds(pl.multiple_of(core * HALF + zz * SHARE, SHARE), SHARE)
@@ -611,33 +587,23 @@
 
     for zz in range(NZ):
         spread(c, zz)
-    for i in (0,) + ORDER[::-1]:
-        src = ring(i)
-        remote(
-            fin.at[other, src], fin.at[other, src], p_ssem.at[i], p_rsem.at[src], ep, partner
-        ).wait_recv()
-        spread(other, src)
+    remote(fin.at[other], fin.at[other], p_ssem, p_rsem, ep, partner).wait_recv()
+    for zz in range(NZ):
+        spread(other, zz)
 
     for copy in swaps:
         copy.wait_send()
-    remote(
-        hv_recv.at[0 : N_TP - 1], hv_recv.at[0 : N_TP - 1], hv_ssem, hv_rsem.at[0], ep, partner
-    ).wait_send()
-    for i in ORDER:
-        scatter_copy(rs_send, rs_recv, rs_ssem, rs_rsem, i).wait_send()
-        ag_copy(i, z).wait_send()
-        scatter_copy(rs2_send, rs2_recv, rs2_ssem, rs2_rsem, i).wait_send()
-        f_copy(i).wait_send()
-        p_copy(ring(i), i).wait_send()
-    p_copy(z, 0).wait_send()
+    remote(all_heads, all_heads, hv_ssem, hv_rsem, ep, partner).wait_send()
+    scatter_all(rs_recv, rs_ssem, rs_rsem).wait_send()
+    scatter_all(rs2_recv, rs2_ssem, rs2_rsem).wait_send()
+    scatter_all(after, ag_ssem, rs_rsem).wait_send()
+    scatter_all(rs_recv, f_ssem, rs_rsem).wait_send()
+    remote(fin.at[other], fin.at[other], p_ssem, p_rsem, ep, partner).wait_send()
     to_partner.wait_send()
-    sent = pl.ds(0, OTHERS * CAP)
-    for n, span in enumerate(spans(OUT_GROUPS)):
-        part_of = disp.at[sent, pl.ds(*span)]
-        remote(part_of, part_of, x_ssem.at[n], x_rsem.at[n, 0], ep, partner).wait_send()
-    for n, span in enumerate(spans(BACK_GROUPS)):
-        part_of = yin.at[sent, pl.ds(*span)]
-        remote(part_of, part_of, y_ssem.at[n], y_rsem.at[n, 0], ep, partner).wait_send()
+    for n in range(len(OUT_GROUPS)):
+        x_all(n).wait_send()
+    for n in range(len(BACK_GROUPS)):
+        y_all(n).wait_send()
 
 
 def write_out(a, b, c, a_out, b_out, c_out, sem):
@@ -718,7 +684,6 @@
             pltpu.VMEM((SLOTS, ROWS), BF16),
             pltpu.VMEM((SLOTS, HALF), BF16),
             pltpu.VMEM((2, N_EP * CAP, HALF), BF16),
-            pltpu.VMEM((N_EP * CAP, D), BF16),
             pltpu.VMEM((2, N_EP * CAP, HALF), BF16),
             pltpu.VMEM((SLOTS, HALF), BF16),
             pltpu.VMEM((2 * ROWS, SLOTS), BF16),
@@ -727,27 +692,28 @@
             pltpu.VMEM((2, NZ, ROWS, SHARE), BF16),
             pltpu.VMEM((1, D), F32),
             pltpu.VMEM((SEQS, KV, LEN), BF16),
-            dma((32,)),
+            pltpu.VMEM((2, H, LEN), F32),
+            dma((21,)),
             dma((4,)),
             dma((4,)),
             dma,
-            dma((N_TP,)),
+            dma,
+            dma,
+            dma,
+            dma,
+            dma((len(OUT_GROUPS),)),
+            dma,
+            dma,
+            dma((len(OUT_GROUPS),)),
+            dma((len(OUT_GROUPS),)),
+            dma((len(BACK_GROUPS),)),
+            dma((len(BACK_GROUPS),)),
+            dma,
+            dma,
+            dma,
             dma((NZ,)),
-            dma((NZ,)),
-            dma((NZ,)),
-            dma((NZ,)),
-            dma,
-            dma,
-            dma((len(OUT_GROUPS),)),
-            dma((len(OUT_GROUPS), 2 * N_EP)),
-            dma((len(BACK_GROUPS),)),
-            dma((len(BACK_GROUPS), 2 * N_EP)),
-            dma((NZ,)),
-            dma((NZ,)),
-            dma((NZ,)),
-            dma((NZ,)),
-            dma((NZ,)),
-            dma((NZ,)),
+            dma,
+            dma,
         ],
         compiler_params=pltpu.CompilerParams(
             collective_id=0, has_side_effects=True, vmem_limit_bytes=60 * 1024 * 1024

time: 60.8 us -> 56.1 us (0.923)
  Pallas kernels: 60.1 us -> 55.4 us
    pallas_call x1, Pallas kernels: 59.3 us -> 54.6 us  [on_device(): pl.pallas_call(kernel, out_shape=(pltpu.VMEM((ROWS, D), BF16), pltpu.VMEM...]
where the time goes in v3:
time: 56.1 us; the launch traced here: 56 us
  Pallas kernels  55.4 us (99%)
  between operations  0.65 us (1%)
    pallas_call x1, Pallas kernels, on_device(): pl.pallas_call(kernel, out_shape=(pltpu.VMEM((ROWS, D), BF16), pltpu.VMEM...  54.6 us

profile of v3, /device:TPU:1, one launch (start us, length us, event | category | flops | bytes accessed | tf_op | source)
XLA Modules:
  0.0 56.0 jit_solution(1205058673917339870)
XLA Ops:
  0.6 54.6 %shard_map.202 = (bf16[64,2048]{1,0:T(8,128)(2,1)S(1)}, bf16[4,256]{1,0:T(4,128)(2,1)S(1)}, bf16[4,32]{1,0:T(4,128)(2,1)S(1)}) custom-call(bf16[64,2048]{1,0:T(8,128)(2,1)} %residual.1, bf16[4,2048,256]{2,1,0:T(8,128)(2,1)} %cache_latent.1, bf16[4,32,2048]{2,1,0:T(8,128)(2,1)} %cache_rope.1, s32[4]{0:T(128)} %lengths_in.1, bf16[4,32,256]{2,1,0:T(8,128)(2,1)} %query_latent.1, ...), custom_call_target="tpu_custom_call" | custom-call | tf_op jit(solution)/shard_map/pallas_call | solution.py:645
  55.3 0.7 %shard_map.203 = (bf16[64,2048]{1,0:T(8,128)(2,1)}, bf16[4,256]{1,0:T(4,128)(2,1)}, bf16[4,32]{1,0:T(4,128)(2,1)}) custom-call(bf16[64,2048]{1,0:T(8,128)(2,1)S(1)} %get-tuple-element.6.a, bf16[4,256]{1,0:T(4,128)(2,1)S(1)} %get-tuple-element.7.b, bf16[4,32]{1,0:T(4,128)(2,1)S(1)} %get-tuple-element.8.c), custom_call_target="tpu_custom_call" | custom-call | tf_op jit(solution)/shard_map/pallas_call | solution.py:742

commit v4 on v3

--- a/solution.py
+++ b/solution.py
@@ -409,7 +409,7 @@
             after.at[z], after.at[z], ag_ssem, ag_rsem.at[group_of(NZ - i)], ep, ring(i) * 2 + c
         )
 
-    for i in ORDER:
+    for i in reversed(ORDER):
         ag_copy(i).start()
 
     mine = pl.ds(pl.multiple_of((ep * 2 + c) * CAP, CAP), CAP)

time: 56.1 us -> 55.5 us (0.989)
  Pallas kernels: 55.4 us -> 54.8 us
    pallas_call x1, Pallas kernels: 54.6 us -> 54 us  [on_device(): pl.pallas_call(kernel, out_shape=(pltpu.VMEM((ROWS, D), BF16), pltpu.VMEM...]
where the time goes in v4:
time: 55.5 us; the launch traced here: 55.4 us
  Pallas kernels  54.8 us (99%)
  between operations  0.65 us (1%)
    pallas_call x1, Pallas kernels, on_device(): pl.pallas_call(kernel, out_shape=(pltpu.VMEM((ROWS, D), BF16), pltpu.VMEM...  54 us

profile of v4, /device:TPU:1, one launch (start us, length us, event | category | flops | bytes accessed | tf_op | source)
XLA Modules:
  0.0 55.4 jit_solution(13534519718180796948)
XLA Ops:
  0.6 54.0 %shard_map.202 = (bf16[64,2048]{1,0:T(8,128)(2,1)S(1)}, bf16[4,256]{1,0:T(4,128)(2,1)S(1)}, bf16[4,32]{1,0:T(4,128)(2,1)S(1)}) custom-call(bf16[64,2048]{1,0:T(8,128)(2,1)} %residual.1, bf16[4,2048,256]{2,1,0:T(8,128)(2,1)} %cache_latent.1, bf16[4,32,2048]{2,1,0:T(8,128)(2,1)} %cache_rope.1, s32[4]{0:T(128)} %lengths_in.1, bf16[4,32,256]{2,1,0:T(8,128)(2,1)} %query_latent.1, ...), custom_call_target="tpu_custom_call" | custom-call | tf_op jit(solution)/shard_map/pallas_call | solution.py:645
  54.7 0.7 %shard_map.203 = (bf16[64,2048]{1,0:T(8,128)(2,1)}, bf16[4,256]{1,0:T(4,128)(2,1)}, bf16[4,32]{1,0:T(4,128)(2,1)}) custom-call(bf16[64,2048]{1,0:T(8,128)(2,1)S(1)} %get-tuple-element.6.a, bf16[4,256]{1,0:T(4,128)(2,1)S(1)} %get-tuple-element.7.b, bf16[4,32]{1,0:T(4,128)(2,1)S(1)} %get-tuple-element.8.c), custom_call_target="tpu_custom_call" | custom-call | tf_op jit(solution)/shard_map/pallas_call | solution.py:742
